TPU v7x, 128 devices: a whole 4x4x4 slice. The times are simulated.
128 devices in a mesh: sp: 16 (over z, y), tp: 8 (over x, core).
Axes of the slice: x: 4, y: 4, z: 4, core: 2. Of those that a mesh axis runs over, the one named last changes fastest.
Arguments:
- skip_stream_vector: bfloat16 [16384, 2048], P(('sp', 'tp')), may hold values from -6 to 6
- probe_preactivation: bfloat16 [16384, 1024], P('sp', 'tp'), may hold values from -6 to 6
- retention_preactivation: bfloat16 [16384, 1024], P('sp', 'tp'), may hold values from -4.5 to 4.5
- content_vector: bfloat16 [16384, 1024], P('sp', 'tp'), may hold values from -6 to 6
- emission_preactivation: bfloat16 [16384, 1024], P('sp', 'tp'), may hold values from -6 to 6
- retention_slack: float32 [1024], P('tp'), may hold values from 0 to 0.12
- surge_rate: float32 [16384, 1024], P('sp', 'tp'), may hold values from -1.2 to 0
- subspace_scaling_factor: float32 [1024], P('tp'), may hold values from 0.1 to 1.9
- emission_matrix: bfloat16 [1024, 2048], replicated, may hold values from -0.1875 to 0.1875
- mlp_scaling_factor: float32 [2048], replicated, may hold values from 0.1 to 1.9
- switch_matrix: bfloat16 [2048, 5632], P('sp', 'tp'), may hold values from -0.125 to 0.125
- expansion_matrix: bfloat16 [2048, 5632], P('sp', 'tp'), may hold values from -0.125 to 0.125
- contraction_matrix: bfloat16 [5632, 2048], P('tp', 'sp'), may hold values from -0.078125 to 0.078125
Outputs:
- stream_out: bfloat16 [16384, 2048], P(('sp', 'tp'))
All inputs are finite; a program needn't handle non-finite values.
Results may differ from a plain program's by a relative error of at most 0.017.
Values may be sent and summed in bfloat16 or wider, within the bound.
A program may use at most 128 MiB of HBM per device.

v0:
```python
import jax
import jax.numpy as jnp
from jax import lax
from jax.sharding import Mesh
from jax.sharding import PartitionSpec as P

HEAD_DIM = 128
BLOCK = 64
TP = ("tp_0", "tp_1")
SP_TP = ("sp", "tp_0", "tp_1")


EPSILON = 1e-06
TOP_PRECISION = lax.Precision.HIGHEST


def in_one_piece(arrays, axis, dim, along):
    both = jnp.concatenate(arrays, axis=along)
    whole, at, outs = (lax.all_gather(both, axis, axis=dim, tiled=True), 0, [])
    for a in arrays:
        outs.append(lax.slice_in_dim(whole, at, at + a.shape[along], axis=along))
        at += a.shape[along]
    return tuple(outs)


def from_everyone(value, axis):
    peers = lax.axis_size(axis)
    return lax.all_to_all(
        jnp.broadcast_to(value[None], (peers, *value.shape)), axis, 0, 0, tiled=True
    )


def all_in_one(value, axis):
    leaves = jax.tree.leaves(value)
    order = sorted(range(len(leaves)), key=lambda k: -leaves[k].size)
    width = (1, *leaves[order[0]].shape)[-1]
    lines = [
        jnp.pad(leaves[k].reshape(-1), (0, -leaves[k].size % width)).reshape(-1, width)
        for k in order
    ]
    both, at, found = (from_everyone(jnp.concatenate(lines), axis), 0, {})
    for k, line in zip(order, lines):
        piece = both[:, at : at + len(line)].reshape(len(both), -1)
        found[k] = piece[:, : leaves[k].size].reshape(-1, *leaves[k].shape)
        at += len(line)
    numbers = iter(range(len(leaves)))
    return jax.tree.map(lambda _: found[next(numbers)], value)


def joined_by_halves(pieces, combine):
    while len(jax.tree.leaves(pieces)[0]) > 1:
        pieces = jax.vmap(combine)(
            *(jax.tree.map(lambda part: part[side::2], pieces) for side in (0, 1))
        )
    return jax.tree.map(lambda part: part[0], pieces)


def carried_in(value, axis, combine, identity):
    peers, here = (lax.axis_size(axis), lax.axis_index(axis))
    passed = jnp.arange(peers) < here

    def kept(part, zero, own):
        part = jnp.where(
            passed.reshape(-1, *(1 for _ in own.shape)),
            part.astype(own.dtype),
            jnp.asarray(zero, own.dtype),
        )
        return part

    pieces = all_in_one(
        jax.tree.map(lambda part, kind: part.astype(kind), value, (jnp.bfloat16, jnp.bfloat16)),
        axis,
    )
    return joined_by_halves(jax.tree.map(kept, pieces, identity, value), combine)


def joined_along(tiles, dim):
    lengths = list(tiles.shape[1:])
    lengths[dim] *= tiles.shape[0]
    return jnp.moveaxis(tiles, 0, dim).reshape(lengths)


def gathered_by_axis(value, axes, dim):
    far, near = axes
    tiles = from_everyone(from_everyone(value, far), near)
    return joined_along(tiles.swapaxes(0, 1).reshape(-1, *value.shape), dim)


def in_blocks(value, dim, peers):
    lengths = value.shape
    tiles = value.reshape(*lengths[:dim], peers, lengths[dim] // peers, *lengths[dim + 1 :])
    return jnp.moveaxis(tiles, dim, 0)


def summed_on_arrival(value, axis, dim):
    tiles = in_blocks(value, dim, lax.axis_size(axis))
    arrived = lax.all_to_all(tiles, axis, split_axis=0, concat_axis=0, tiled=True)
    return arrived.astype(jnp.float32).sum(axis=0)


def sum_by_axis(value, axes, dim):
    far, near = axes
    own = summed_on_arrival(in_blocks(value, dim, lax.axis_size(far)), near, dim + 1)
    return jnp.sum(
        lax.all_to_all(own.astype(jnp.bfloat16), far, 0, 0, tiled=True).astype(jnp.float32), axis=0
    )


def block_step(carry, inputs):
    memory_state, offsets = carry
    query_block, input_gate_block, value_block, log_blk = inputs
    cumulative_decay = jnp.cumsum(log_blk, axis=1)
    length = log_blk.shape[1]
    carried_share = jnp.einsum(
        "eia,eax->eix",
        query_block * jnp.exp(cumulative_decay),
        memory_state,
        precision=TOP_PRECISION,
    )
    middle = cumulative_decay[:, length // 2, :][:, None, :]
    left_side = query_block * jnp.exp(cumulative_decay - middle)
    right_side = input_gate_block * jnp.exp(middle - cumulative_decay)
    causal = (jnp.arange(length)[:, None] >= jnp.arange(length)[None, :])[None, :, :]
    scores = jnp.einsum("htk,hsk->hts", left_side, right_side, precision=TOP_PRECISION)
    scores = jnp.where(causal, scores, 0.0)
    outputs = carried_share + jnp.einsum(
        "hts,hsv->htv", scores, value_block, precision=TOP_PRECISION
    )
    closing_log_decay = cumulative_decay[:, -1, :]
    updated_memory_state = jnp.exp(closing_log_decay)[:, :, None] * memory_state + jnp.einsum(
        "qnj,qnl->qjl",
        input_gate_block * jnp.exp(closing_log_decay[:, None, :] - cumulative_decay),
        value_block,
        precision=TOP_PRECISION,
    )
    return (
        (updated_memory_state, offsets + closing_log_decay),
        (outputs, cumulative_decay + offsets[:, None, :]),
    )


def split_blocks(values, heads_here):
    count = values.shape[0]
    return values.reshape(count // BLOCK, BLOCK, heads_here, HEAD_DIM).transpose(0, 2, 1, 3)


def admission_source_matrix(
    probe_preactivation, retention_preactivation, content_vector, retention_slack, surge_rate
):
    query_act = jax.nn.silu(probe_preactivation.astype(jnp.float32))
    admission_factor = retention_slack[None, :] * jax.nn.sigmoid(
        -retention_preactivation.astype(jnp.float32)
    )
    retention_logarithm = jnp.log1p(-admission_factor) + surge_rate
    return (query_act, admission_factor, content_vector.astype(jnp.float32), retention_logarithm)


def head_output(outputs, subspace_scaling_factor, emission_preactivation):
    count, heads_here = (outputs.shape[0], outputs.shape[1])
    squares = jnp.mean(outputs * outputs, axis=-1, keepdims=True)
    scaled = (
        outputs
        * lax.rsqrt(squares + EPSILON)
        * subspace_scaling_factor.reshape(heads_here, HEAD_DIM)
    )
    scaled = scaled.reshape(count, heads_here * HEAD_DIM)
    return (scaled * jax.nn.silu(emission_preactivation.astype(jnp.float32))).astype(jnp.bfloat16)


def row_norm(stream, mlp_scaling_factor):
    streamf = stream.astype(jnp.float32)
    squares = jnp.mean(streamf * streamf, axis=-1, keepdims=True)
    return (streamf * lax.rsqrt(squares + EPSILON) * mlp_scaling_factor).astype(jnp.bfloat16)


def chain(earlier, later):
    return (earlier[0] * later[0], later[0][:, :, None] * earlier[1] + later[1])


def on_device(
    skip_stream_vector,
    probe_preactivation,
    retention_preactivation,
    content_vector,
    emission_preactivation,
    retention_slack,
    surge_rate,
    subspace_scaling_factor,
    emission_matrix,
    mlp_scaling_factor,
    switch_matrix,
    expansion_matrix,
    contraction_matrix,
):
    gate_whole, up_whole = in_one_piece((switch_matrix, expansion_matrix), "sp", 0, 1)
    down_whole = lax.all_gather(contraction_matrix, "sp", axis=1, tiled=True)
    heads_here = probe_preactivation.shape[1] // HEAD_DIM
    tok_rows = probe_preactivation.shape[0]
    arranged_sources = admission_source_matrix(
        probe_preactivation, retention_preactivation, content_vector, retention_slack, surge_rate
    )
    block_list = tuple((split_blocks(item, heads_here) for item in arranged_sources))
    start_carry = (
        jnp.zeros((heads_here, HEAD_DIM, HEAD_DIM), jnp.float32),
        jnp.zeros((heads_here, HEAD_DIM), jnp.float32),
    )
    (memory_state, offsets), (outputs, cumulative_log_decay) = lax.scan(
        block_step, start_carry, block_list
    )
    incoming_state = carried_in(
        (jnp.exp(offsets), memory_state),
        "sp",
        chain,
        (jnp.ones_like(offsets), jnp.zeros_like(memory_state)),
    )
    outputs = outputs + jnp.einsum(
        "jmxo,mos->jmxs",
        block_list[0] * jnp.exp(cumulative_log_decay),
        incoming_state[1],
        precision=TOP_PRECISION,
    )
    outputs = outputs.transpose(0, 2, 1, 3).reshape(tok_rows, heads_here, HEAD_DIM)
    mixed = head_output(outputs, subspace_scaling_factor, emission_preactivation)
    regrouped = lax.all_to_all(mixed, TP, split_axis=0, concat_axis=1, tiled=True)
    projected = jnp.dot(regrouped, emission_matrix, preferred_element_type=jnp.float32)
    stream = (skip_stream_vector.astype(jnp.float32) + projected).astype(jnp.bfloat16)
    normed = row_norm(stream, mlp_scaling_factor)
    all_rows = gathered_by_axis(normed, ("tp_0", "tp_1"), 0)
    gate_proj = jnp.dot(all_rows, gate_whole, preferred_element_type=jnp.float32)
    up_proj = jnp.dot(all_rows, up_whole, preferred_element_type=jnp.float32)
    hidden = (jax.nn.silu(gate_proj) * up_proj).astype(jnp.bfloat16)
    partial_sum = jnp.dot(hidden, down_whole, preferred_element_type=jnp.float32)
    summed = sum_by_axis(partial_sum.astype(jnp.bfloat16), ("tp_0", "tp_1"), 0)
    return (stream.astype(jnp.float32) + summed).astype(jnp.bfloat16)


def solution(mesh):
    split = Mesh(mesh.devices.reshape(mesh.shape["sp"], 4, 2), ("sp", "tp_0", "tp_1"))
    return jax.shard_map(
        on_device,
        mesh=split,
        in_specs=(
            P(SP_TP, None),
            P("sp", TP),
            P("sp", TP),
            P("sp", TP),
            P("sp", TP),
            P(TP),
            P("sp", TP),
            P(TP),
            P(),
            P(),
            P("sp", TP),
            P("sp", TP),
            P(TP, "sp"),
        ),
        out_specs=P(SP_TP, None),
        check_vma=False,
    )
```

profile of v0, /device:TPU:0, one launch (start us, length us, event | category | flops | bytes accessed | tf_op | source)
XLA Modules:
  0.0 193.7 jit_solution(10395686392634396452)
XLA Ops:
  6.5 1.8 pad_maximum_fusion
  8.4 1.1 convert_multiply_fusion.1
  9.5 1.0 convert.2
  10.5 1.5 divide_multiply_fusion
  12.0 17.0 %while.17 = (s32[]{:T(128)}, f32[1,128,128]{2,1,0:T(8,128)S(1)}, f32[1,128]{1,0:T(1,128)S(1)}, f32[16,1,64,128]{3,2,1,0:T(8,128)S(1)}, f32[16,1,64,128]{3,2,1,0:...) while((s32[]{:T(128)}, f32[1,128,128]{2,1,0:T(8,128)S(1)}, ...), condition=%wide.region_2.3_spmd.clone, body=%wide.region_0.2_spmd.clone.sunk | while | flops 38412544 | bytes 879768 | solution.py:207
  29.0 0.9 broadcast_in_dim.48
  29.9 8.2 %all-to-all-start = ((bf16[16,129,128]{2,1,0:T(8,128)(2,1)}), bf16[16,129,128]{2,1,0:T(8,128)(2,1)S(1)}, u32[]{:S(2)}, u32[]{:S(2)}) async-start(bf16[16,129,128]{2,1,0:T(8,128)(2,1)} %broadcast_in_dim.48), calls=%async_computation | async-start | bytes 1114112 | tf_op jit(solution)/shard_map/all_to_all | solution.py:28
  38.1 0.7 all-gather.5.cloned.1.call-update
  38.9 11.2 %all-to-all-done = bf16[16,129,128]{2,1,0:T(8,128)(2,1)S(1)} async-done(((bf16[16,129,128]{2,1,0:T(8,128)(2,1)}), bf16[16,129,128]{2,1,0:T(8,128)(2,1)S(1)}, u32[]{:S(2)}, u32[]{:S(2)}) %all-to-all-start) | async-done | bytes 528416 | tf_op jit(solution)/shard_map/all_to_all | solution.py:28
  50.8 0.7 multiply_reduce_fusion.1
  51.9 11.6 %all_to_all.44 = bf16[8,128,128]{2,1,0:T(8,128)(2,1)S(1)} all-to-all(bf16[8,128,128]{2,1,0:T(8,128)(2,1)S(1)} %bitcast.185), channel_id=1, replica_groups=mesh['sp'=16,'tp_0'=4,'tp_1'=2] {'tp_0','tp_1'}, dimensions={0} | all-to-all | bytes 524288 | tf_op jit(solution)/shard_map/all_to_all | solution.py:224
  63.7 3.0 %multiply_reduce_fusion = (f32[128]{0:T(128)S(1)}, f32[128,2048]{1,0:T(8,128)S(1)}) fusion(bf16[128,1024]{0,1:T(8,128)(2,1)S(1)} %bitcast.183, bf16[1024,2048]{1,0:T(8,128)(2,1)} %param.23, bf16[128,2048]{1,0:T(8,128)(2,1)S(1)} %copy-done), kind=kOutput, calls=%fused_computation.66 | convolution fusion | flops 538443648 | bytes 6029824 | tf_op jit(solution)/shard_map/dot_general | solution.py:225
  67.1 28.8 %all_to_all.45 = bf16[4,128,2048]{2,1,0:T(8,128)(2,1)S(1)} all-to-all(bf16[4,128,2048]{2,1,0:T(8,128)(2,1)S(1)} %broadcast_in_dim.74), channel_id=1, replica_groups=mesh['sp'=16,'tp_0'=4,'tp_1'=2] {'tp_0'}, dimensions={0} | all-to-all | bytes 4194304 | tf_op jit(solution)/shard_map/all_to_all | solution.py:28
  95.9 0.5 broadcast_in_dim.75
  96.5 7.1 %all_to_all.46 = bf16[2,4,128,2048]{3,2,1,0:T(8,128)(2,1)S(1)} all-to-all(bf16[2,4,128,2048]{3,2,1,0:T(8,128)(2,1)S(1)} %broadcast_in_dim.75), channel_id=1, replica_groups=mesh['sp'=16,'tp_0'=4,'tp_1'=2] {'tp_1'}, dimensions={0} | all-to-all | bytes 8388608 | tf_op jit(solution)/shard_map/all_to_all | solution.py:28
  103.6 2.3 %copy.36 = bf16[2,4,128,2048]{3,2,0,1:T(8,128)(2,1)} copy(bf16[2,4,128,2048]{3,2,1,0:T(8,128)(2,1)S(1)} %all_to_all.46) | data formatting | bytes 8388608 | tf_op jit(solution)/shard_map/all_to_all | solution.py:28
  105.9 7.9 %fusion.43 = f32[1024,704]{0,1:T(8,128)} fusion(bf16[1024,2048]{1,0:T(8,128)(2,1)} %bitcast.178, bf16[2048,1408]{0,1:T(8,128)(2,1)} %all-gather.3.cloned.1.call-done), kind=kOutput, calls=%fused_computation.56 | convolution fusion | flops 2952790016 | bytes 9961472 | tf_op jit(solution)/shard_map/dot_general | solution.py:229
  113.8 14.8 %all-gather.5.cloned.1.call-done = bf16[704,2048]{1,0:T(8,128)(2,1)} async-done(((bf16[704,128]{1,0:T(8,128)(2,1)}), bf16[704,2048]{1,0:T(8,128)(2,1)}) %all-gather.5.cloned.1.call-update) | async-done | bytes 2883600 | tf_op jit(solution)/shard_map/all_gather | solution.py:196
  128.6 12.1 %convolution_convert_fusion = bf16[1024,2048]{1,0:T(8,128)(2,1)} fusion(bf16[704,2048]{1,0:T(8,128)(2,1)} %all-gather.5.cloned.1.call-done, f32[1024,704]{0,1:T(8,128)} %fusion.43, bf16[1024,2048]{1,0:T(8,128)(2,1)} %bitcast.179, bf16[2048,1408]{0,1:T(8,128)(2,1)} %all-gather.3.cloned.1.call-done), kind=kOutput, calls=%fused_computation.53 | convolution fusion | flops 5912002560 | bytes 17039360 | tf_op jit(solution)/shard_map/dot_general | solution.py:232
  140.7 2.5 %copy.39 = bf16[4,2,128,2048]{3,2,0,1:T(8,128)(2,1)S(1)} copy(bf16[4,2,128,2048]{3,2,1,0:T(8,128)(2,1)} %bitcast.180) | data formatting | bytes 8388608 | tf_op jit(solution)/shard_map/reshape;reshape | solution.py:91
  143.2 8.2 %all_to_all.47 = bf16[2,4,128,2048]{3,2,1,0:T(8,128)(2,1)} all-to-all(bf16[2,4,128,2048]{3,2,1,0:T(8,128)(2,1)S(1)} %bitcast.177), channel_id=1, replica_groups=mesh['sp'=16,'tp_0'=4,'tp_1'=2] {'tp_1'}, dimensions={0} | all-to-all | bytes 8388608 | tf_op jit(solution)/shard_map/all_to_all | solution.py:97
  151.3 3.5 %reduce_sum.41 = bf16[4,128,2048]{2,1,0:T(8,128)(2,1)S(1)} reduce(bf16[2,4,128,2048]{3,2,1,0:T(8,128)(2,1)} %all_to_all.47, bf16[]{:T(256)} %constant.49.clone.1), dimensions={0}, to_apply=%region_5.6 | reduce | flops 1048576 | bytes 6291458 | tf_op jit(solution)/shard_map/reduce_sum | solution.py:98
  154.9 30.7 %all_to_all.48 = bf16[4,128,2048]{2,1,0:T(8,128)(2,1)S(1)} all-to-all(bf16[4,128,2048]{2,1,0:T(8,128)(2,1)S(1)} %reduce_sum.41), channel_id=1, replica_groups=mesh['sp'=16,'tp_0'=4,'tp_1'=2] {'tp_0'}, dimensions={0} | all-to-all | bytes 4194304 | tf_op jit(solution)/shard_map/all_to_all | solution.py:105
  186.0 0.9 add_convert_fusion
  (197 shorter events, 18.0 us)
Async XLA Ops:
  6.5 99.4 %all-gather.3.cloned.1.call-start = ((), (), s32[]{:S(2)}) async-start(), calls=%async_computation.6 | async-start | bytes 6127616 | tf_op jit(solution)/shard_map/all_gather | solution.py:19
  29.9 20.2 %all-to-all-start = ((bf16[16,129,128]{2,1,0:T(8,128)(2,1)}), bf16[16,129,128]{2,1,0:T(8,128)(2,1)S(1)}, u32[]{:S(2)}, u32[]{:S(2)}) async-start(bf16[16,129,128]{2,1,0:T(8,128)(2,1)} %broadcast_in_dim.48), calls=%async_computation | async-start | bytes 1114112 | tf_op jit(solution)/shard_map/all_to_all | solution.py:28
  38.1 90.5 %all-gather.5.cloned.1.call-start = ((), (), s32[]{:S(2)}) async-start(), calls=%async_computation.7 | async-start | bytes 3063808 | tf_op jit(solution)/shard_map/all_gather | solution.py:196
  50.3 1.3 copy-start.1
  50.3 1.3 copy-start.3
  50.6 13.1 %copy-start = (bf16[128,2048]{1,0:T(8,128)(2,1)S(1)}, bf16[128,2048]{1,0:T(8,128)(2,1)}, u32[]{:S(2)}) copy-start(bf16[128,2048]{1,0:T(8,128)(2,1)} %param.15) | copy-start | bytes 1572868
  63.7 3.0 %copy-start.2 = (f32[2048]{0:T(1024)S(1)}, f32[2048]{0:T(1024)}, u32[]{:S(2)}) copy-start(f32[2048]{0:T(1024)} %param.24) | copy-start | bytes 24580
Sparse Core Ops, SparseCore 0:
  9.4 66.9 all-gather.2
  78.6 49.9 all-gather.4
where the time goes:
time: 194 us
  blocking collectives  86.3 us (44%)
  matrix products  37.4 us (19%)
  waiting for transfers between devices  26.8 us (14%)
  between operations  13.7 us (7%)
  other arithmetic  13.2 us (7%)
  starting transfers between devices  8.21 us (4%)
  local copies, waits for them, and re-layouts  7.13 us (4%)
    all_to_all x2, blocking collectives, from_everyone(): lax.all_to_all(jnp.broadcast_to(value[None], (peers, *value.shape)), axis...  35.9 us
    all_to_all x1, blocking collectives, sum_by_axis(): lax.all_to_all(own.astype(jnp.bfloat16), far, 0, 0, tiled=True)  30.7 us
    all_gather x1, waiting for transfers between devices, on_device(): down_whole = lax.all_gather(contraction_matrix, 'sp', axis=1, tiled=True)  14.8 us
    dot_general x1, matrix products, on_device(): jnp.dot(hidden, down_whole, preferred_element_type=jnp.float32)  12.1 us
    all_to_all x1, blocking collectives, on_device(): lax.all_to_all(mixed, TP, split_axis=0, concat_axis=1, tiled=True)  11.6 us
    all_to_all x1, waiting for transfers between devices, from_everyone(): lax.all_to_all(jnp.broadcast_to(value[None], (peers, *value.shape)), axis...  11.2 us
    all_to_all x1, blocking collectives, summed_on_arrival(): lax.all_to_all(tiles, axis, split_axis=0, concat_axis=0, tiled=True)  8.18 us
    all_to_all x1, starting transfers between devices, from_everyone(): lax.all_to_all(jnp.broadcast_to(value[None], (peers, *value.shape)), axis...  8.16 us
  transfers between devices with their start and end apart: 3, of which 2 were waited for; matrix products, arithmetic and copies ran while one was open for 19% of the time, Pallas kernels for 0%

commit v1 on v0

v1 whole, which is shorter than its diff:
```python
import functools

import jax
import jax.numpy as jnp
from jax import lax
from jax.experimental import pallas as pl
from jax.experimental.pallas import tpu as pltpu
from jax.sharding import Mesh
from jax.sharding import PartitionSpec as P

MESH = pl.DeviceIdType.MESH
F32 = jnp.float32
BF16 = jnp.bfloat16
EPSILON = 1e-06
HD = 128
BLOCK = 64
TOK = 1024
ROWS = 512
D = 2048
GU, DOWN = 0, 1
PLUS = {GU: +1, DOWN: -1}


def wrap(value, n=4):
    return lax.rem(value + n, n)


def nt(a, b):
    return lax.dot_general(a, b, (((1,), (1,)), ((), ())), preferred_element_type=F32)


def tn(a, b):
    return lax.dot_general(a, b, (((0,), (0,)), ((), ())), preferred_element_type=F32)


def mm(a, b):
    return jnp.dot(a, b, preferred_element_type=F32)


def kernel(
    skip_ref, q_ref, r_ref, v_ref, e_ref, slack_ref, surge_ref, gain_ref, emission_ref,
    norm_gain_ref, gate_ref, up_ref, down_ref,
    out_ref,
    W, DN, EB, SK, MX, MIXS, STREAM, NORM, ACC, HID, SSQ, RES,
    CUM, IG, DS, SB, ST, STR, SIN, OL, QC, GT,
    OPPS, OPPR, OWN, PN, NBS, NBR,
    w_recv, w_side, w_send, state_recv, state_send, skip_sem, skip_send, mix_recv, mix_send,
    e_sem, opp_recv, opp_send, nb_recv, nb_send,
):
    z, y, x, c = (lax.axis_index(name) for name in ("z", "y", "x", "c"))
    sp = z * 4 + y
    other = 1 - c
    sends = []

    barrier = pltpu.get_barrier_semaphore()
    for k in range(1, 16):
        to = lax.rem(sp + k, 16)
        pl.semaphore_signal(barrier, inc=1, device_id={"z": to // 4, "y": lax.rem(to, 4)}, device_id_type=MESH)
    for step in (1, -1):
        for core in (0, 1):
            pl.semaphore_signal(barrier, inc=1, device_id={"x": wrap(x + step), "c": jnp.int32(core)}, device_id_type=MESH)
    pl.semaphore_signal(barrier, inc=1, device_id={"c": other}, device_id_type=MESH)

    loads = [
        pltpu.make_async_copy(emission_ref.at[:, pl.ds(n * 256, 256)], EB.at[n], e_sem.at[n])
        for n in range(8)
    ]
    for load in loads:
        load.start()

    own_rows = pl.ds(pl.multiple_of(sp * 128, 128), 128)
    for j in range(5):
        W[c, own_rows, j * 256 : j * 256 + 128] = gate_ref[:, j * 128 : (j + 1) * 128]
        W[c, own_rows, j * 256 + 128 : (j + 1) * 256] = up_ref[:, j * 128 : (j + 1) * 128]
    W[c, own_rows, 1280:1408] = jnp.concatenate([gate_ref[:, 640:704], up_ref[:, 640:704]], axis=1)
    DN[c, sp] = down_ref[...]
    SK[x] = skip_ref[...]

    pl.semaphore_wait(barrier, 20)

    AXES = {0: ("y", "z"), 1: ("z", "y")}
    here = {"z": z, "y": y}

    def unit(kind, color, core, rel):
        origin = wrap(z + rel["z"]) * 4 + wrap(y + rel["y"])
        if kind == GU:
            start = pl.multiple_of(origin * 128 + color * 64, 64)
            return W.at[core, pl.ds(start, 64), :]
        return DN.at[core, origin, pl.ds(color * 352, 352), :]

    def number(rel):
        return (rel["z"] % 4) * 4 + rel["y"] % 4

    counter = [0]

    def push(kind, color, rel, axis, step):
        there = dict(rel)
        there[axis] = rel[axis] - step
        ref = unit(kind, color, c, rel)
        copy = pltpu.make_async_remote_copy(
            src_ref=ref, dst_ref=ref,
            send_sem=w_send.at[counter[0]],
            recv_sem=w_recv.at[kind, color, number(there)],
            device_id={axis: wrap(here[axis] + step)}, device_id_type=MESH,
        )
        counter[0] += 1
        copy.start()
        sends.append(copy)

    def side(kind, color, rel):
        ref = unit(kind, color, c, rel)
        copy = pltpu.make_async_remote_copy(
            src_ref=ref, dst_ref=ref,
            send_sem=w_send.at[counter[0]],
            recv_sem=w_side.at[kind, color, number(rel)],
            device_id={"c": other}, device_id_type=MESH,
        )
        counter[0] += 1
        copy.start()
        sends.append(copy)

    def arrived(kind, color, rel):
        ref = unit(kind, color, c, rel)
        pltpu.make_async_copy(ref, ref, w_recv.at[kind, color, number(rel)]).wait()

    def side_arrived(kind, color, rel):
        ref = unit(kind, color, other, rel)
        pltpu.make_async_copy(ref, ref, w_side.at[kind, color, number(rel)]).wait()

    def at(color, first, second):
        one, two = AXES[color]
        return {one: first, two: second}

    def turn(kind, second_offset):
        return PLUS[kind] * {0: 1, -1: -1, 1: 1, 2: -1}[second_offset]

    def stage(kind, n):
        for color in (0, 1):
            one, two = AXES[color]
            own = at(color, 0, 0)
            if n == 0:
                for step in (1, -1):
                    push(kind, color, own, one, step)
            elif n == 1:
                for step in (1, -1):
                    push(kind, color, own, two, step)
                side(kind, color, own)
        if n == 2:
            for f in (-1, 1):
                for color in (0, 1):
                    one, two = AXES[color]
                    rel = at(color, f, 0)
                    arrived(kind, color, rel)
                    if PLUS[kind] == -f:
                        push(kind, color, rel, one, -f)
                    for step in (1, -1):
                        push(kind, color, rel, two, step)
                    side(kind, color, rel)
        if n == 4:
            for color in (0, 1):
                two = AXES[color][1]
                rel = at(color, 2, 0)
                arrived(kind, color, rel)
                for step in (1, -1):
                    push(kind, color, rel, two, step)
                side(kind, color, rel)
        for first in {3: (0,), 5: (-1, 1), 6: (2,)}.get(n, ()):
            for s in (-1, 1):
                for color in (0, 1):
                    two = AXES[color][1]
                    rel = at(color, first, s)
                    arrived(kind, color, rel)
                    if turn(kind, first) == -s:
                        push(kind, color, rel, two, -s)
                    side(kind, color, rel)
        for first in {5: (0,), 6: (-1, 1), 7: (2,)}.get(n, ()):
            for color in (0, 1):
                rel = at(color, first, 2)
                arrived(kind, color, rel)
                side(kind, color, rel)

    stage(GU, 0)

    def skip_copy(source, slot, rows, sem, count, step):
        return pltpu.make_async_remote_copy(
            src_ref=source, dst_ref=SK.at[slot, rows, :],
            send_sem=skip_send.at[count], recv_sem=skip_sem.at[sem],
            device_id={"x": wrap(x + step)}, device_id_type=MESH,
        )

    for i, step in enumerate((1, -1)):
        copy = skip_copy(skip_ref, x, pl.ds(0, 128), i, i, step)
        copy.start()
        sends.append(copy)

    def skip_arrived(slot, rows, sem):
        ref = SK.at[slot, rows, :]
        pltpu.make_async_copy(ref, ref, skip_sem.at[sem]).wait()

    def skip_relay():
        left, right = wrap(x - 1), wrap(x + 1)
        first, second = pl.ds(0, 64), pl.ds(64, 64)
        skip_arrived(left, pl.ds(0, 128), 0)
        copy = skip_copy(SK.at[left, first, :], left, first, 2, 2, 1)
        copy.start()
        sends.append(copy)
        skip_arrived(right, pl.ds(0, 128), 1)
        copy = skip_copy(SK.at[right, second, :], right, second, 3, 3, -1)
        copy.start()
        sends.append(copy)

    i256 = lax.broadcasted_iota(jnp.int32, (256, 256), 0)
    j256 = lax.broadcasted_iota(jnp.int32, (256, 256), 1)
    causal = jnp.logical_and(i256 >= j256, i256 // BLOCK == j256 // BLOCK)
    triangle = jnp.where(causal, 1.0, 0.0).astype(BF16)
    upper_half = lax.broadcasted_iota(jnp.int32, (128, 128), 0) < BLOCK
    closings = []
    for s in range(4):
        rows = slice(s * 256, (s + 1) * 256)
        ig = slack_ref[...] * jax.nn.sigmoid(-r_ref[rows].astype(F32))
        lf = jnp.log1p(-ig) + surge_ref[rows]
        high = lf.astype(BF16)
        rest = lf - high.astype(F32)
        mid = rest.astype(BF16)
        low = (rest - mid.astype(F32)).astype(BF16)
        parts = mm(triangle, jnp.concatenate([high, mid, low], axis=1))
        cum = parts[:, :128] + parts[:, 128:256] + parts[:, 256:]
        CUM[rows] = cum
        IG[rows] = ig
        blocks = cum.reshape(4, BLOCK, HD)
        last = blocks[:, BLOCK - 1 : BLOCK, :]
        closings += [last[b] for b in range(4)]
        keys = (ig * jnp.exp(last - blocks).reshape(256, HD)).astype(BF16)
        for p in range(2):
            pair = keys[p * 128 : (p + 1) * 128]
            none = jnp.zeros_like(pair)
            both = jnp.concatenate(
                [jnp.where(upper_half, pair, none), jnp.where(upper_half, none, pair)], axis=1
            )
            grown = tn(v_ref[s * 256 + p * 128 : s * 256 + (p + 1) * 128], both)
            DS[s * 4 + p * 2] = grown[:, :128]
            DS[s * 4 + p * 2 + 1] = grown[:, 128:]
    state = jnp.zeros((HD, HD), F32)
    passed = jnp.zeros((1, HD), F32)
    offsets = []
    for b in range(16):
        SB[b] = state.astype(BF16)
        offsets.append(passed)
        state = state * jnp.exp(closings[b]) + DS[b]
        passed = passed + closings[b]
    ST[0:128] = state.astype(BF16)
    high = passed.astype(BF16)
    rest = passed - high.astype(F32)
    mid = rest.astype(BF16)
    low = (rest - mid.astype(F32)).astype(BF16)
    which = lax.broadcasted_iota(jnp.int32, (16, HD), 0)
    ST[128:144] = jnp.where(
        which == 0, high.astype(F32), jnp.where(which == 1, mid.astype(F32), jnp.where(which == 2, low.astype(F32), 0.0))
    ).astype(BF16)

    def state_copy(k):
        to = sp + k
        return pltpu.make_async_remote_copy(
            src_ref=ST, dst_ref=STR.at[k - 1],
            send_sem=state_send.at[k - 1], recv_sem=state_recv.at[k - 1],
            device_id={"z": to // 4, "y": lax.rem(to, 4)}, device_id_type=MESH,
        )

    for k in range(15, 0, -1):

        @pl.when(sp + k < 16)
        def _():
            state_copy(k).start()

    stage(GU, 1)

    for s in range(4):
        rows = slice(s * 256, (s + 1) * 256)
        q = q_ref[rows].astype(F32)
        qa = q * jax.nn.sigmoid(q)
        cum = CUM[rows]
        ig = IG[rows]
        blocks = cum.reshape(4, BLOCK, HD)
        middle = blocks[:, BLOCK // 2 : BLOCK // 2 + 1, :]
        centred = (blocks - middle).reshape(256, HD)
        left = (qa * jnp.exp(centred)).astype(BF16)
        right = (ig * jnp.exp(-centred)).astype(BF16)
        scores = jnp.where(causal, nt(left, right), 0.0).astype(BF16)
        local = mm(scores, v_ref[rows])
        faded = qa * jnp.exp(cum)
        before = jnp.concatenate([offsets[s * 4 + b].reshape(1, 1, HD) for b in range(4)], axis=0)
        QC[rows] = (qa * jnp.exp(blocks + before).reshape(256, HD)).astype(BF16)
        faded = faded.astype(BF16)
        for p in range(2):
            pair = faded[p * 128 : (p + 1) * 128]
            none = jnp.zeros_like(pair)
            both = jnp.concatenate(
                [jnp.where(upper_half, pair, none), jnp.where(upper_half, none, pair)], axis=1
            )
            b = s * 4 + p * 2
            carried = nt(both, jnp.concatenate([SB[b], SB[b + 1]], axis=1))
            OL[s * 256 + p * 128 : s * 256 + (p + 1) * 128] = local[p * 128 : (p + 1) * 128] + carried
        emission = e_ref[rows].astype(F32)
        GT[rows] = gain_ref[...] * emission * jax.nn.sigmoid(emission)

    stage(GU, 2)
    skip_relay()

    SIN[0:128] = jnp.zeros((HD, HD), F32)
    SIN[128:136] = jnp.zeros((8, HD), F32)
    for k in range(1, 16):

        @pl.when(sp >= k)
        def _():
            ref = STR.at[k - 1]
            pltpu.make_async_copy(ref, ref, state_recv.at[k - 1]).wait()
            since = SIN[128:129]
            SIN[0:128] = SIN[0:128] + STR[k - 1, 0:128].astype(F32) * jnp.exp(since)
            tail = STR[k - 1, 128:144].astype(F32)
            SIN[128:129] = since + (tail[0:1] + tail[1:2] + tail[2:3])

    incoming = SIN[0:128].astype(BF16)
    for s in range(4):
        rows = slice(s * 256, (s + 1) * 256)
        o = OL[rows] + nt(QC[rows], incoming)
        squares = jnp.mean(o * o, axis=-1, keepdims=True)
        mixed = (o * lax.rsqrt(squares + EPSILON) * GT[rows]).astype(BF16)
        for core in (0, 1):
            MIXS[core, s * 128 : (s + 1) * 128] = mixed[core * 128 : (core + 1) * 128]

    head = x * 2 + c
    MX[head] = MIXS[c]

    def mix_copy(source, slab, sem, count, device):
        copy = pltpu.make_async_remote_copy(
            src_ref=source, dst_ref=MX.at[slab],
            send_sem=mix_send.at[count], recv_sem=mix_recv.at[sem],
            device_id=device, device_id_type=MESH,
        )
        copy.start()
        sends.append(copy)

    count = 0
    for i, step in enumerate((1, -1)):
        for core in (0, 1):
            mix_copy(MIXS.at[core], head, i * 2 + c, count, {"x": wrap(x + step), "c": jnp.int32(core)})
            count += 1
    mix_copy(MIXS.at[other], head, 4, count, {"c": other})
    count += 1

    def mix_arrived(slab, sem):
        ref = MX.at[slab]
        pltpu.make_async_copy(ref, ref, mix_recv.at[sem]).wait()

    stage(GU, 3)
    left, right = wrap(x - 1), wrap(x + 1)
    mix_arrived(left * 2, 0)
    mix_copy(MX.at[left * 2], left * 2, 5, count, {"x": right})
    mix_arrived(right * 2 + 1, 3)
    mix_copy(MX.at[right * 2 + 1], right * 2 + 1, 6, count + 1, {"x": left})
    stage(GU, 4)
    for load in loads:
        load.wait()
    opposite = wrap(x + 2)
    skip_arrived(opposite, pl.ds(0, 64), 2)
    skip_arrived(opposite, pl.ds(64, 64), 3)
    mix_arrived(left * 2 + 1, 1)
    mix_arrived(right * 2, 2)
    mix_arrived(x * 2 + other, 4)
    stage(GU, 5)
    mix_arrived(opposite * 2, 5)
    mix_arrived(opposite * 2 + 1, 6)

    SSQ[...] = jnp.zeros((ROWS, 128), F32)

    def project(n, carry):
        mixed = jnp.concatenate([MX[h] for h in range(8)], axis=1)
        skipped = SK[:, :, pl.ds(pl.multiple_of(n * 256, 256), 256)].reshape(ROWS, 256)
        stream = (skipped.astype(F32) + mm(mixed, EB[n])).astype(BF16)
        STREAM[n] = stream
        wide = stream.astype(F32)
        wide = wide * wide
        SSQ[...] += wide[:, :128] + wide[:, 128:]
        return carry

    lax.fori_loop(0, 8, project, 0)
    scale = lax.rsqrt(jnp.sum(SSQ[...], axis=1, keepdims=True) * (1.0 / D) + EPSILON)

    for n in range(8):
        gain = norm_gain_ref[:, n * 256 : (n + 1) * 256]
        NORM[n] = (STREAM[n].astype(F32) * scale * gain).astype(BF16)

    stage(DOWN, 0)
    stage(DOWN, 1)

    GROUPS = (0, -1, 1, 2)

    def await_sides(kind, dz):
        for dy in (0, -1, 1, 2):
            for color in (0, 1):
                side_arrived(kind, color, {"z": dz, "y": dy})

    lane = lax.broadcasted_iota(jnp.int32, (ROWS, 128), 1)

    def silu(a):
        return a * jax.nn.sigmoid(a)

    def gate_up(index, dz):
        plane = wrap(z + dz)
        deep = pl.ds(pl.multiple_of(plane * 512, 512), 512)

        def take(acc):
            if index == 0:
                return acc
            return None

        def partial(weights):
            rows = jnp.concatenate([NORM[plane * 2], NORM[plane * 2 + 1]], axis=1)
            return mm(rows, weights)

        def tile(t, carry):
            h = t // 5
            columns = pl.ds(pl.multiple_of(lax.rem(t, 5) * 256, 256), 256)
            part = partial(W[h, deep, columns])
            if index > 0:
                part = part + ACC[t]
            if index < 3:
                ACC[t] = part
            else:
                HID[t] = (silu(part[:, :128]) * part[:, 128:]).astype(BF16)
            return carry

        lax.fori_loop(0, 10, tile, 0)
        part = partial(jnp.concatenate([W[0, deep, 1280:1408], W[1, deep, 1280:1408]], axis=1))
        if index > 0:
            part = part + ACC[10]
        if index < 3:
            ACC[10] = part
        else:
            a, b = part[:, :128], part[:, 128:]
            gates = jnp.where(lane < 64, a, pltpu.roll(b, 64, 1))
            ups = jnp.where(lane < 64, pltpu.roll(a, 64, 1), b)
            HID[10] = (silu(gates) * ups).astype(BF16)

    await_sides(GU, 0)
    gate_up(0, 0)
    stage(GU, 6)
    await_sides(GU, -1)
    gate_up(1, -1)
    await_sides(GU, 1)
    stage(GU, 7)
    stage(DOWN, 2)
    gate_up(2, 1)
    await_sides(GU, 2)
    stage(DOWN, 3)
    gate_up(3, 2)
    stage(DOWN, 4)
    stage(DOWN, 5)

    def chunk(xi):
        return pl.ds(pl.multiple_of(xi * 128, 128), 128)

    def down(index, dz):
        plane = wrap(z + dz)

        def pair(p, carry):
            def block(yy):
                at_column = plane * 4 + p * 2 + yy
                return jnp.concatenate(
                    [DN[0, at_column, 0:640], DN[1, at_column, 0:640],
                     DN[0, at_column, 640:704], DN[1, at_column, 640:704]], axis=0,
                )

            weights = jnp.concatenate([block(0), block(1)], axis=1)
            hidden = jnp.concatenate([HID[t] for t in range(11)], axis=1)
            RES[...] = mm(hidden, weights)
            OPPS[index, p] = RES[chunk(opposite)].astype(BF16)
            OWN[index, p] = RES[chunk(x)]
            PN[0, index, p] = RES[chunk(right)]
            PN[1, index, p] = RES[chunk(left)]
            return carry

        lax.fori_loop(0, 2, pair, 0)
        for p, step in enumerate((1, -1)):
            copy = pltpu.make_async_remote_copy(
                src_ref=OPPS.at[index, p], dst_ref=OPPR.at[index, p],
                send_sem=opp_send.at[index, p], recv_sem=opp_recv.at[index, p],
                device_id={"x": wrap(x + step)}, device_id_type=MESH,
            )
            copy.start()
            sends.append(copy)

    def hand_on(index):
        for p, step in enumerate((1, -1)):
            ref = OPPR.at[index, p]
            pltpu.make_async_copy(ref, ref, opp_recv.at[index, p]).wait()
            NBS[p, index, p] = (PN[p, index, p] + OPPR[index, p].astype(F32)).astype(BF16)
            NBS[p, index, 1 - p] = PN[p, index, 1 - p].astype(BF16)
            copy = pltpu.make_async_remote_copy(
                src_ref=NBS.at[p, index], dst_ref=NBR.at[p, index],
                send_sem=nb_send.at[p, index], recv_sem=nb_recv.at[p, index],
                device_id={"x": wrap(x + step)}, device_id_type=MESH,
            )
            copy.start()
            sends.append(copy)

    def finish(index, dz):
        plane = wrap(z + dz)
        for p in range(2):
            ref = NBR.at[p, index]
            pltpu.make_async_copy(ref, ref, nb_recv.at[p, index]).wait()
        for p in range(2):
            summed = OWN[index, p] + NBR[0, index, p].astype(F32) + NBR[1, index, p].astype(F32)
            stream = STREAM[plane * 2 + p, chunk(x)].astype(F32)
            columns = pl.ds(pl.multiple_of(plane * 512 + p * 256, 256), 256)
            out_ref[:, columns] = (stream + summed).astype(BF16)

    await_sides(DOWN, 0)
    down(0, 0)
    stage(DOWN, 6)
    await_sides(DOWN, -1)
    down(1, -1)
    hand_on(0)
    await_sides(DOWN, 1)
    down(2, 1)
    hand_on(1)
    stage(DOWN, 7)
    await_sides(DOWN, 2)
    down(3, 2)
    hand_on(2)
    hand_on(3)
    for index, dz in enumerate(GROUPS):
        finish(index, dz)

    for copy in sends:
        copy.wait_send()
    for k in range(15, 0, -1):

        @pl.when(sp + k < 16)
        def _():
            state_copy(k).wait_send()


def on_device(skip, q, r, v, e, slack, surge, gain, emission, norm_gain, gate, up, down):
    vmem = pl.BlockSpec(memory_space=pltpu.VMEM)
    dma = pltpu.SemaphoreType.DMA
    return pl.pallas_call(
        kernel,
        out_shape=jax.ShapeDtypeStruct((128, D), BF16),
        in_specs=[vmem] * 8 + [pl.BlockSpec(memory_space=pl.ANY)] + [vmem] * 4,
        out_specs=vmem,
        scratch_shapes=[
            pltpu.VMEM((2, D, 1408), BF16),
            pltpu.VMEM((2, 16, 704, 128), BF16),
            pltpu.VMEM((8, 1024, 256), BF16),
            pltpu.VMEM((4, 128, D), BF16),
            pltpu.VMEM((8, ROWS, 128), BF16),
            pltpu.VMEM((2, ROWS, 128), BF16),
            pltpu.VMEM((8, ROWS, 256), BF16),
            pltpu.VMEM((8, ROWS, 256), BF16),
            pltpu.VMEM((11, ROWS, 256), F32),
            pltpu.VMEM((11, ROWS, 128), BF16),
            pltpu.VMEM((ROWS, 128), F32),
            pltpu.VMEM((ROWS, 256), F32),
            pltpu.VMEM((TOK, HD), F32),
            pltpu.VMEM((TOK, HD), F32),
            pltpu.VMEM((16, HD, HD), F32),
            pltpu.VMEM((16, HD, HD), BF16),
            pltpu.VMEM((144, HD), BF16),
            pltpu.VMEM((15, 144, HD), BF16),
            pltpu.VMEM((136, HD), F32),
            pltpu.VMEM((TOK, HD), F32),
            pltpu.VMEM((TOK, HD), BF16),
            pltpu.VMEM((TOK, HD), F32),
            pltpu.VMEM((4, 2, 128, 256), BF16),
            pltpu.VMEM((4, 2, 128, 256), BF16),
            pltpu.VMEM((4, 2, 128, 256), F32),
            pltpu.VMEM((2, 4, 2, 128, 256), F32),
            pltpu.VMEM((2, 4, 2, 128, 256), BF16),
            pltpu.VMEM((2, 4, 2, 128, 256), BF16),
            dma((2, 2, 16)),
            dma((2, 2, 16)),
            dma((124,)),
            dma((15,)),
            dma((15,)),
            dma((4,)),
            dma((4,)),
            dma((7,)),
            dma((7,)),
            dma((8,)),
            dma((4, 2)),
            dma((4, 2)),
            dma((2, 4)),
            dma((2, 4)),
        ],
        compiler_params=pltpu.CompilerParams(
            collective_id=0, has_side_effects=True, vmem_limit_bytes=67043328
        ),
        name="layer",
    )(
        skip, q, r, v, e, slack.reshape(1, -1), surge, gain.reshape(1, -1), emission,
        norm_gain.reshape(1, -1), gate, up, down,
    )


def solution(mesh):
    split = Mesh(mesh.devices.reshape(4, 4, 4, 2), ("z", "y", "x", "c"))
    sp, tp = ("z", "y"), ("x", "c")
    return jax.shard_map(
        on_device,
        mesh=split,
        in_specs=(
            P(sp + tp, None),
            P(sp, tp),
            P(sp, tp),
            P(sp, tp),
            P(sp, tp),
            P(tp),
            P(sp, tp),
            P(tp),
            P(),
            P(),
            P(sp, tp),
            P(sp, tp),
            P(tp, sp),
        ),
        out_specs=P(sp + tp, None),
        check_vma=False,
    )
```

time: 194 us -> 98.6 us (0.51)
  Pallas kernels: 0 us -> 91.7 us
  blocking collectives: 86.3 us -> 0 us
  matrix products: 37.4 us -> 0 us
  waiting for transfers between devices: 26.8 us -> 0 us
  between operations: 13.7 us -> 0.01 us
  other arithmetic: 13.2 us -> 0 us
  starting transfers between devices: 8.21 us -> 0 us
    pallas_call x0 -> x1, Pallas kernels: none -> 91.7 us  [on_device(): pl.pallas_call(kernel, out_shape=jax.ShapeDtypeStruct((128, D), BF16), in...]
    all_to_all x5 -> x0, blocking collectives: 86.3 us -> none  [the longest x2 35.9 us: from_everyone(): lax.all_to_all(jnp.broadcast_to(value[None], (peers, *value.shape)), axis...]
    dot_general x68 -> x0, matrix products: 37.4 us -> none  [the longest x1 12.1 us: on_device(): jnp.dot(hidden, down_whole, preferred_element_type=jnp.float32)]
    all_gather x2 -> x0, waiting for transfers between devices: 14.8 us -> none  [the longest x1 14.8 us: on_device(): down_whole = lax.all_gather(contraction_matrix, 'sp', axis=1, tiled=True)]
    all_to_all x1 -> x0, waiting for transfers between devices: 11.2 us -> none  [from_everyone(): lax.all_to_all(jnp.broadcast_to(value[None], (peers, *value.shape)), axis...]
    all_to_all x1 -> x0, starting transfers between devices: 8.16 us -> none  [from_everyone(): lax.all_to_all(jnp.broadcast_to(value[None], (peers, *value.shape)), axis...]
    unnamed x8 -> x3, local copies, waits for them, and re-layouts: 0.03 us -> 5.35 us
    reduce_sum x2 -> x0, other arithmetic: 3.93 us -> none  [the longest x1 3.55 us: summed_on_arrival(): return arrived.astype(jnp.float32).sum(axis=0)]
  transfers between devices with their start and end apart: 3 -> 0, of which waited for: 2 -> 0; matrix products, arithmetic and copies ran while one was open for 19% -> 0% of each run, Pallas kernels for 0% -> 0%
where the time goes in v1:
time: 98.6 us; the launch traced here: 97.1 us
  Pallas kernels  91.7 us (93%)
  local copies, waits for them, and re-layouts  5.35 us (5%)
    pallas_call x1, Pallas kernels, on_device(): pl.pallas_call(kernel, out_shape=jax.ShapeDtypeStruct((128, D), BF16), in...  91.7 us
    unnamed x3, local copies, waits for them, and re-layouts  5.35 us

profile of v1, /device:TPU:0, one launch (start us, length us, event | category | flops | bytes accessed | tf_op | source)
XLA Modules:
  0.0 97.1 jit_solution(5289831002516667895)
XLA Ops:
  0.0 1.7 %copy.14.gate_ref = bf16[128,704]{1,0:T(8,128)(2,1)} copy(bf16[128,704]{0,1:T(8,128)(2,1)} %param.23) | data formatting | bytes 360448 | tf_op args[10]
  1.7 1.7 %copy.15.up_ref = bf16[128,704]{1,0:T(8,128)(2,1)} copy(bf16[128,704]{0,1:T(8,128)(2,1)} %param.24) | data formatting | bytes 360448 | tf_op args[11]
  3.5 91.7 %layer.1 = bf16[128,2048]{1,0:T(8,128)(2,1)} custom-call(bf16[128,2048]{1,0:T(8,128)(2,1)} %skip_ref.1, bf16[1024,128]{1,0:T(8,128)(2,1)} %q_ref.1, bf16[1024,128]{1,0:T(8,128)(2,1)} %r_ref.1, bf16[1024,128]{1,0:T(8,128)(2,1)} %v_ref.1, bf16[1024,128]{1,0:T(8,128)(2,1)} %e_ref.1, f32[1,128]{1,0:T(1,128)} %bitcast.4, f32[1024,128]{1,0:T(8,128)} %surge_ref.1, ...), custom_call_target="tpu_custom_call" | custom-call | tf_op jit(solution)/shard_map/layer/pallas_call | solution.py:547
  95.2 1.9 %copy.17 = bf16[128,2048]{1,0:T(8,128)(2,1)} copy(bf16[128,2048]{1,0:T(8,128)(2,1)} %layer.1) | data formatting | bytes 1048576

commit v2 on v1

v2 whole, which is shorter than its diff:
```python
import functools

import jax
import jax.numpy as jnp
from jax import lax
from jax.experimental import pallas as pl
from jax.experimental.pallas import tpu as pltpu
from jax.sharding import Mesh
from jax.sharding import PartitionSpec as P

MESH = pl.DeviceIdType.MESH
F32 = jnp.float32
BF16 = jnp.bfloat16
EPSILON = 1e-06
HD = 128
BLOCK = 64
TOK = 1024
ROWS = 512
D = 2048
GU, DOWN = 0, 1
PLUS = {GU: +1, DOWN: -1}


def wrap(value, n=4):
    return lax.rem(value + n, n)


def nt(a, b):
    return lax.dot_general(a, b, (((1,), (1,)), ((), ())), preferred_element_type=F32)


def tn(a, b):
    return lax.dot_general(a, b, (((0,), (0,)), ((), ())), preferred_element_type=F32)


def mm(a, b):
    return jnp.dot(a, b, preferred_element_type=F32)


def kernel(
    skip_in, q_in, r_in, v_in, e_in, slack_in, surge_in, gain_in, emission_ref,
    norm_gain_in, gate_in, up_in, down_in,
    out_ref,
    skip_ref, QE, RV, slack_ref, surge_ref, gain_ref, norm_gain_ref, OWNED,
    W, DN, EB, SK, MX, MIXS, STREAM, NORM, ACC, HID, SSQ, RES,
    CUM, IG, DS, SB, STR, TOT, OL, QC, GT,
    OPPS, OPPR, OWN, PN, NBS, NBR,
    w_recv, side_gu, side_down, w_send, state_recv, state_send, total_recv, total_send,
    skip_sem, skip_send, mix_recv, mix_send, e_sem, in_sem, opp_recv, opp_send, nb_recv, nb_send,
):
    z, y, x, c = (lax.axis_index(name) for name in ("z", "y", "x", "c"))
    sp = z * 4 + y
    other = 1 - c
    q_ref, e_ref, r_ref, v_ref = QE.at[0], QE.at[1], RV.at[0], RV.at[1]
    gate_ref, up_ref, down_ref = (OWNED.at[i] for i in range(3))

    def arrive(ref, sem):
        pltpu.make_async_copy(ref, ref, sem).wait()

    barrier = pltpu.get_barrier_semaphore()
    for k in range(1, 4):
        pl.semaphore_signal(barrier, inc=1, device_id={"y": wrap(y + k)}, device_id_type=MESH)
        pl.semaphore_signal(barrier, inc=1, device_id={"z": wrap(z + k)}, device_id_type=MESH)
    for step in (1, -1):
        for core in (0, 1):
            pl.semaphore_signal(barrier, inc=1, device_id={"x": wrap(x + step), "c": jnp.int32(core)}, device_id_type=MESH)
    pl.semaphore_signal(barrier, inc=1, device_id={"c": other}, device_id_type=MESH)

    def load(source, target, sem):
        pltpu.make_async_copy(source, target, in_sem.at[sem]).start()

    load(gate_in, gate_ref, 0)
    load(up_in, up_ref, 0)
    load(down_in, down_ref, 0)
    load(r_in, r_ref, 1)
    load(v_in, v_ref, 1)
    load(surge_in, surge_ref, 2)
    load(slack_in, slack_ref, 3)
    load(skip_in, skip_ref, 4)
    load(q_in, q_ref, 5)
    load(e_in, e_ref, 5)
    load(gain_in, gain_ref, 6)
    load(norm_gain_in, norm_gain_ref, 7)
    for n in range(8):
        source = emission_ref.at[:, pl.ds(n * 256, 256)]
        pltpu.make_async_copy(source, EB.at[n], e_sem.at[0]).start()

    arrive(OWNED, in_sem.at[0])
    own_rows = pl.ds(pl.multiple_of(c * D + sp * 128, 128), 128)
    for j in range(5):
        W[own_rows, j * 256 : j * 256 + 128] = gate_ref[j * 128 : (j + 1) * 128].T
        W[own_rows, j * 256 + 128 : (j + 1) * 256] = up_ref[j * 128 : (j + 1) * 128].T
    W[own_rows, 1280:1408] = jnp.concatenate([gate_ref[640:704], up_ref[640:704]], axis=0).T
    DN[c * 16 + sp] = down_ref[...]
    arrive(RV, in_sem.at[1])
    arrive(surge_ref, in_sem.at[2])
    arrive(slack_ref, in_sem.at[3])

    i256 = lax.broadcasted_iota(jnp.int32, (256, 256), 0)
    j256 = lax.broadcasted_iota(jnp.int32, (256, 256), 1)
    causal = jnp.logical_and(i256 >= j256, i256 // BLOCK == j256 // BLOCK)
    triangle = jnp.where(causal, 1.0, 0.0).astype(BF16)
    upper_half = lax.broadcasted_iota(jnp.int32, (128, 128), 0) < BLOCK
    closings = []
    for s in range(4):
        rows = slice(s * 256, (s + 1) * 256)
        ig = slack_ref[...] * jax.nn.sigmoid(-r_ref[rows].astype(F32))
        lf = jnp.log1p(-ig) + surge_ref[rows]
        high = lf.astype(BF16)
        rest = lf - high.astype(F32)
        mid = rest.astype(BF16)
        low = (rest - mid.astype(F32)).astype(BF16)
        parts = mm(triangle, jnp.concatenate([high, mid, low], axis=1))
        cum = parts[:, :128] + parts[:, 128:256] + parts[:, 256:]
        CUM[rows] = cum
        IG[rows] = ig
        blocks = cum.reshape(4, BLOCK, HD)
        last = blocks[:, BLOCK - 1 : BLOCK, :]
        closings += [last[b] for b in range(4)]
        keys = (ig * jnp.exp(last - blocks).reshape(256, HD)).astype(BF16)
        for p in range(2):
            pair = keys[p * 128 : (p + 1) * 128]
            none = jnp.zeros_like(pair)
            both = jnp.concatenate(
                [jnp.where(upper_half, pair, none), jnp.where(upper_half, none, pair)], axis=1
            )
            grown = tn(v_ref[s * 256 + p * 128 : s * 256 + (p + 1) * 128], both)
            DS[s * 4 + p * 2] = grown[:, :128]
            DS[s * 4 + p * 2 + 1] = grown[:, 128:]
    state = jnp.zeros((HD, HD), F32)
    passed = jnp.zeros((1, HD), F32)
    offsets = []
    for b in range(16):
        SB[b] = state.astype(BF16)
        offsets.append(passed)
        state = state * jnp.exp(closings[b]) + DS[b]
        passed = passed + closings[b]
    STR[0, 0:128] = state.astype(BF16)
    which = lax.broadcasted_iota(jnp.int32, (16, HD), 0)

    def spread(value):
        high = value.astype(BF16)
        rest = value - high.astype(F32)
        mid = rest.astype(BF16)
        low = rest - mid.astype(F32)
        rows = jnp.where(which == 2, low, 0.0)
        rows = jnp.where(which == 1, mid.astype(F32), rows)
        return jnp.where(which == 0, high.astype(F32), rows).astype(BF16)

    def joined(rows):
        rows = rows.astype(F32)
        return rows[0:1] + rows[1:2] + rows[2:3]

    STR[0, 128:144] = spread(passed)

    pl.semaphore_wait(barrier, 11)

    for k in range(1, 4):
        pltpu.make_async_remote_copy(
            src_ref=STR.at[0], dst_ref=STR.at[k],
            send_sem=state_send.at[0], recv_sem=state_recv.at[k - 1],
            device_id={"y": wrap(y + k)}, device_id_type=MESH,
        ).start()

    AXES = {0: ("y", "z"), 1: ("z", "y")}
    ORDER = (
        (0, 0), (1, 0), (-1, 0), (0, 1), (0, -1), (2, 0), (0, 2), (1, 1),
        (-1, -1), (1, -1), (-1, 1), (2, 1), (2, -1), (1, 2), (-1, 2), (2, 2),
    )
    here = {"z": z, "y": y}

    def short(offset):
        return (offset + 1) % 4 - 1

    def unit(kind, color, rel):
        origin = wrap(z + rel["z"]) * 4 + wrap(y + rel["y"])
        if kind == GU:
            start = pl.multiple_of(c * D + origin * 128 + color * 64, 64)
            return W.at[pl.ds(start, 64), :]
        return DN.at[c * 16 + origin, pl.ds(color * 352, 352), :]

    def units(kind, count):
        return W.at[pl.ds(0, 64 * count), :] if kind == GU else DN.at[pl.ds(0, count // 2)]

    counts = {GU: 0, DOWN: 0}

    def lot(kind, color, rel):
        one, two = AXES[color]
        first, second = short(rel[one]), short(rel[two])
        if second == 0:
            return {-PLUS[kind]: 0, PLUS[kind]: 1, 2: 3}[first]
        if second == 2:
            return {0: 6, -1: 8, 1: 8, 2: 9}[first]
        return {0: 2, -1: 4, 1: 5, 2: 7}[first]

    LOTS = (2, 2, 4, 2, 4, 4, 2, 4, 4, 2)

    def arrived(kind, number):
        arrive(units(kind, LOTS[number]), w_recv.at[kind, number])

    def start_unit(kind, color, rel, recv_sem, device):
        ref = unit(kind, color, rel)
        pltpu.make_async_remote_copy(
            src_ref=ref, dst_ref=ref, send_sem=w_send.at[kind], recv_sem=recv_sem,
            device_id=device, device_id_type=MESH,
        ).start()
        counts[kind] += 1

    def push(kind, color, rel, axis, step):
        there = dict(rel)
        there[axis] = rel[axis] - step
        sem = w_recv.at[kind, lot(kind, color, there)]
        start_unit(kind, color, rel, sem, {axis: wrap(here[axis] + step)})

    def side(kind, color, rel):
        place = (short(rel["y"]), short(rel["z"]))
        sem = side_gu.at[place[1] % 4] if kind == GU else side_down.at[ORDER.index(place) // 2]
        start_unit(kind, color, rel, sem, {"c": other})

    def at(color, first, second):
        one, two = AXES[color]
        return {one: first, two: second}

    def turn(kind, second_offset):
        return PLUS[kind] * {0: 1, -1: -1, 1: 1, 2: -1}[second_offset]

    def stage(kind, n):
        if n in (0, 1):
            for color in (0, 1):
                for step in (1, -1):
                    push(kind, color, at(color, 0, 0), AXES[color][n], step)
                if n == 1:
                    side(kind, color, at(color, 0, 0))
        if n == 2:
            f = -PLUS[kind]
            arrived(kind, 0)
            for color in (0, 1):
                push(kind, color, at(color, f, 0), AXES[color][0], -f)
        for number, f in {2: ((0, -PLUS[kind]), (1, PLUS[kind])), 4: ((3, 2),)}.get(n, ()):
            if number > 0:
                arrived(kind, number)
            for color in (0, 1):
                for step in (1, -1):
                    push(kind, color, at(color, f, 0), AXES[color][1], step)
                side(kind, color, at(color, f, 0))
        for number, first in {3: ((2, 0),), 5: ((4, -1), (5, 1)), 6: ((7, 2),)}.get(n, ()):
            arrived(kind, number)
            for s in (-1, 1):
                for color in (0, 1):
                    if turn(kind, first) == -s:
                        push(kind, color, at(color, first, s), AXES[color][1], -s)
            for s in (-1, 1):
                for color in (0, 1):
                    side(kind, color, at(color, first, s))
        for number, firsts in {5: ((6, (0,)),), 6: ((8, (-1, 1)),), 7: ((9, (2,)),)}.get(n, ()):
            arrived(kind, number)
            for first in firsts:
                for color in (0, 1):
                    side(kind, color, at(color, first, 2))

    stage(GU, 0)

    def skip_copy(source, slot, rows, sem, step):
        return pltpu.make_async_remote_copy(
            src_ref=source, dst_ref=SK.at[slot, rows, :],
            send_sem=skip_send.at[0], recv_sem=skip_sem.at[sem],
            device_id={"x": wrap(x + step)}, device_id_type=MESH,
        )

    arrive(skip_ref, in_sem.at[4])
    for i, step in enumerate((1, -1)):
        skip_copy(skip_ref, x, pl.ds(0, 128), i, step).start()

    def skip_arrived(slot, rows, sem):
        arrive(SK.at[slot, rows, :], skip_sem.at[sem])

    def skip_relay():
        left, right = wrap(x - 1), wrap(x + 1)
        first, second = pl.ds(0, 64), pl.ds(64, 64)
        skip_arrived(left, pl.ds(0, 128), 0)
        skip_copy(SK.at[left, first, :], left, first, 2, 1).start()
        skip_arrived(right, pl.ds(0, 128), 1)
        skip_copy(SK.at[right, second, :], right, second, 3, -1).start()

    for k in range(1, 4):
        arrive(STR.at[k], state_recv.at[k - 1])
    plane = jnp.zeros((HD, HD), F32)
    plane_log = jnp.zeros((1, HD), F32)
    before, before_log = plane, plane_log
    for yy in range(4):
        slot = wrap(y - yy)
        before = jnp.where(y == yy, plane, before)
        before_log = jnp.where(y == yy, plane_log, before_log)
        log = joined(STR[slot, 128:144])
        plane = plane * jnp.exp(log) + STR[slot, 0:128].astype(F32)
        plane_log = plane_log + log
    TOT[0, 0:128] = plane.astype(BF16)
    TOT[0, 128:144] = spread(plane_log)

    def total_copy(k):
        return pltpu.make_async_remote_copy(
            src_ref=TOT.at[0], dst_ref=TOT.at[k],
            send_sem=total_send.at[k - 1], recv_sem=total_recv.at[k - 1],
            device_id={"z": wrap(z + k)}, device_id_type=MESH,
        )

    for k in range(1, 4):

        @pl.when(z + k < 4)
        def _():
            total_copy(k).start()

        @pl.when(z < k)
        def _():
            TOT[k] = jnp.zeros((144, HD), BF16)

    stage(GU, 1)
    SK[x] = skip_ref[...]
    arrive(QE, in_sem.at[5])
    arrive(gain_ref, in_sem.at[6])
    arrive(norm_gain_ref, in_sem.at[7])
    for s in range(4):
        rows = slice(s * 256, (s + 1) * 256)
        q = q_ref[rows].astype(F32)
        qa = q * jax.nn.sigmoid(q)
        cum = CUM[rows]
        ig = IG[rows]
        blocks = cum.reshape(4, BLOCK, HD)
        middle = blocks[:, BLOCK // 2 : BLOCK // 2 + 1, :]
        centred = (blocks - middle).reshape(256, HD)
        left = (qa * jnp.exp(centred)).astype(BF16)
        right = (ig * jnp.exp(-centred)).astype(BF16)
        scores = jnp.where(causal, nt(left, right), 0.0).astype(BF16)
        local = mm(scores, v_ref[rows])
        faded = qa * jnp.exp(cum)
        faded_by = jnp.concatenate([offsets[s * 4 + b].reshape(1, 1, HD) for b in range(4)], axis=0)
        QC[rows] = (qa * jnp.exp(blocks + faded_by).reshape(256, HD)).astype(BF16)
        faded = faded.astype(BF16)
        for p in range(2):
            pair = faded[p * 128 : (p + 1) * 128]
            none = jnp.zeros_like(pair)
            both = jnp.concatenate(
                [jnp.where(upper_half, pair, none), jnp.where(upper_half, none, pair)], axis=1
            )
            b = s * 4 + p * 2
            carried = nt(both, jnp.concatenate([SB[b], SB[b + 1]], axis=1))
            OL[s * 256 + p * 128 : s * 256 + (p + 1) * 128] = local[p * 128 : (p + 1) * 128] + carried
        emission = e_ref[rows].astype(F32)
        GT[rows] = gain_ref[...] * emission * jax.nn.sigmoid(emission)

    for k in range(1, 4):

        @pl.when(z >= k)
        def _():
            arrive(TOT.at[k], total_recv.at[k - 1])

    since = before_log
    for k in range(1, 4):
        before = before + TOT[k, 0:128].astype(F32) * jnp.exp(since)
        since = since + joined(TOT[k, 128:144])
    incoming = before.astype(BF16)
    for s in range(4):
        rows = slice(s * 256, (s + 1) * 256)
        o = OL[rows] + nt(QC[rows], incoming)
        squares = jnp.mean(o * o, axis=-1, keepdims=True)
        mixed = (o * lax.rsqrt(squares + EPSILON) * GT[rows]).astype(BF16)
        for core in (0, 1):
            MIXS[core, s * 128 : (s + 1) * 128] = mixed[core * 128 : (core + 1) * 128]

    head = x * 2 + c
    MX[head] = MIXS[c]

    def mix_copy(source, slab, sem, device):
        pltpu.make_async_remote_copy(
            src_ref=source, dst_ref=MX.at[slab],
            send_sem=mix_send.at[0], recv_sem=mix_recv.at[sem],
            device_id=device, device_id_type=MESH,
        ).start()

    for i, step in enumerate((1, -1)):
        for core in (0, 1):
            mix_copy(MIXS.at[core], head, i * 2 + c, {"x": wrap(x + step), "c": jnp.int32(core)})
    mix_copy(MIXS.at[other], head, 4, {"c": other})

    def mix_arrived(slab, sem):
        arrive(MX.at[slab], mix_recv.at[sem])

    stage(GU, 2)
    stage(GU, 3)
    skip_relay()
    stage(GU, 4)
    left, right = wrap(x - 1), wrap(x + 1)
    mix_arrived(left * 2, 0)
    mix_copy(MX.at[left * 2], left * 2, 5, {"x": right})
    mix_arrived(right * 2 + 1, 3)
    mix_copy(MX.at[right * 2 + 1], right * 2 + 1, 6, {"x": left})
    stage(GU, 5)
    arrive(EB, e_sem.at[0])
    opposite = wrap(x + 2)
    skip_arrived(opposite, pl.ds(0, 64), 2)
    skip_arrived(opposite, pl.ds(64, 64), 3)
    mix_arrived(left * 2 + 1, 1)
    mix_arrived(right * 2, 2)
    mix_arrived(x * 2 + other, 4)
    mix_arrived(opposite * 2, 5)
    mix_arrived(opposite * 2 + 1, 6)

    SSQ[...] = jnp.zeros((ROWS, 128), F32)

    def project(n, carry):
        mixed = jnp.concatenate([MX[h] for h in range(8)], axis=1)
        skipped = SK[:, :, pl.ds(pl.multiple_of(n * 256, 256), 256)].reshape(ROWS, 256)
        stream = (skipped.astype(F32) + mm(mixed, EB[n])).astype(BF16)
        STREAM[n] = stream
        wide = stream.astype(F32)
        wide = wide * wide
        SSQ[...] += wide[:, :128] + wide[:, 128:]
        return carry

    lax.fori_loop(0, 8, project, 0)
    scale = lax.rsqrt(jnp.sum(SSQ[...], axis=1, keepdims=True) * (1.0 / D) + EPSILON)

    for n in range(8):
        gain = norm_gain_ref[:, n * 256 : (n + 1) * 256]
        NORM[n] = (STREAM[n].astype(F32) * scale * gain).astype(BF16)

    def await_sides(dz):
        arrive(units(GU, 8), side_gu.at[dz % 4])

    lane = lax.broadcasted_iota(jnp.int32, (ROWS, 128), 1)

    def silu(a):
        return a * jax.nn.sigmoid(a)

    def gate_up(planes, first, last):
        places = [wrap(z + dz) for dz in planes]
        rows = [
            [pl.ds(pl.multiple_of(h * D + p * 512, 512), 512) for p in places] for h in (0, 1)
        ]

        def partial(weights):
            normed = [NORM[p * 2 + i] for p in places for i in (0, 1)]
            return mm(jnp.concatenate(normed, axis=1), jnp.concatenate(weights, axis=0))

        def tile(j, carry):
            columns = pl.ds(pl.multiple_of(j * 256, 256), 256)
            for h in (0, 1):
                t = h * 5 + j
                part = partial([W[deep, columns] for deep in rows[h]])
                if not first:
                    part = part + ACC[t]
                if not last:
                    ACC[t] = part
                else:
                    HID[t] = (silu(part[:, :128]) * part[:, 128:]).astype(BF16)
            return carry

        lax.fori_loop(0, 5, tile, 0)
        part = partial(
            [
                jnp.concatenate([W[one, 1280:1408], W[two, 1280:1408]], axis=1)
                for one, two in zip(*rows)
            ]
        )
        if not first:
            part = part + ACC[10]
        if not last:
            ACC[10] = part
        else:
            a, b = part[:, :128], part[:, 128:]
            gates = jnp.where(lane < 64, a, pltpu.roll(b, 64, 1))
            ups = jnp.where(lane < 64, pltpu.roll(a, 64, 1), b)
            HID[10] = (silu(gates) * ups).astype(BF16)

    def chunk(xi):
        return pl.ds(pl.multiple_of(xi * 128, 128), 128)

    def column_of(i):
        dy, dz = ORDER[i]
        return wrap(z + dz) * 4 + wrap(y + dy)

    def down(i):
        arrive(units(DOWN, 4), side_down.at[i])

        def block(at_column):
            one, two = at_column, 16 + at_column
            return jnp.concatenate(
                [DN[one, 0:640], DN[two, 0:640], DN[one, 640:704], DN[two, 640:704]], axis=0
            )

        weights = jnp.concatenate([block(column_of(2 * i)), block(column_of(2 * i + 1))], axis=1)
        hidden = jnp.concatenate([HID[t] for t in range(11)], axis=1)
        res = RES.at[i % 2]
        res[...] = mm(hidden, weights)
        far = res[chunk(opposite)].astype(BF16)
        for half, step in enumerate((1, -1)):
            OPPS[i, half] = far[:, half * 128 : (half + 1) * 128]
            pltpu.make_async_remote_copy(
                src_ref=OPPS.at[i, half], dst_ref=OPPR.at[i, half],
                send_sem=opp_send.at[0], recv_sem=opp_recv.at[i],
                device_id={"x": wrap(x + step)}, device_id_type=MESH,
            ).start()
        OWN[i] = res[chunk(x)]
        PN[0, i] = res[chunk(right)]
        PN[1, i] = res[chunk(left)]

    def hand_on(i):
        arrive(OPPR.at[i], opp_recv.at[i])
        for half, step in enumerate((1, -1)):
            mine = slice(half * 128, (half + 1) * 128)
            rest = slice(128 - half * 128, 256 - half * 128)
            NBS[i, half, :, mine] = (PN[half, i, :, mine] + OPPR[i, half].astype(F32)).astype(BF16)
            NBS[i, half, :, rest] = PN[half, i, :, rest].astype(BF16)
            pltpu.make_async_remote_copy(
                src_ref=NBS.at[i, half], dst_ref=NBR.at[i, half],
                send_sem=nb_send.at[0], recv_sem=nb_recv.at[i],
                device_id={"x": wrap(x + step)}, device_id_type=MESH,
            ).start()

    def finish(i):
        arrive(NBR.at[i], nb_recv.at[i])
        summed = OWN[i] + NBR[i, 0].astype(F32) + NBR[i, 1].astype(F32)
        for half in (0, 1):
            column = column_of(2 * i + half)
            lanes = pl.ds(pl.multiple_of(lax.rem(column, 2) * 128, 128), 128)
            stream = STREAM[column // 2, chunk(x), lanes].astype(F32)
            columns = pl.ds(pl.multiple_of(column * 128, 128), 128)
            out_ref[:, columns] = (stream + summed[:, half * 128 : (half + 1) * 128]).astype(BF16)

    stage(DOWN, 0)
    await_sides(0)
    gate_up((0,), True, False)
    stage(GU, 6)
    stage(DOWN, 1)
    await_sides(-1)
    await_sides(1)
    gate_up((-1, 1), False, False)
    stage(DOWN, 2)
    stage(GU, 7)
    stage(DOWN, 3)
    await_sides(2)
    gate_up((2,), False, True)
    down(0)
    stage(DOWN, 4)
    down(1)
    stage(DOWN, 5)
    down(2)
    hand_on(0)
    down(3)
    hand_on(1)
    down(4)
    stage(DOWN, 6)
    hand_on(2)
    down(5)
    hand_on(3)
    down(6)
    stage(DOWN, 7)
    hand_on(4)
    down(7)
    hand_on(5)
    finish(0)
    finish(1)
    hand_on(6)
    hand_on(7)
    for i in range(2, 8):
        finish(i)

    for kind in (GU, DOWN):
        arrive(units(kind, counts[kind]), w_send.at[kind])
    arrive(STR.at[pl.ds(0, 3)], state_send.at[0])
    arrive(SK.at[pl.ds(0, 3)], skip_send.at[0])
    arrive(MX.at[pl.ds(0, 7)], mix_send.at[0])
    arrive(OPPS, opp_send.at[0])
    arrive(NBS, nb_send.at[0])
    for k in range(1, 4):

        @pl.when(z + k < 4)
        def _():
            total_copy(k).wait_send()


def on_device(skip, q, r, v, e, slack, surge, gain, emission, norm_gain, gate, up, down):
    vmem = pl.BlockSpec(memory_space=pltpu.VMEM)
    dma = pltpu.SemaphoreType.DMA
    return pl.pallas_call(
        kernel,
        out_shape=jax.ShapeDtypeStruct((128, D), BF16),
        in_specs=[pl.BlockSpec(memory_space=pltpu.HBM)] * 13,
        out_specs=vmem,
        scratch_shapes=[
            pltpu.VMEM((128, D), BF16),
            pltpu.VMEM((2, TOK, HD), BF16),
            pltpu.VMEM((2, TOK, HD), BF16),
            pltpu.VMEM((1, HD), F32),
            pltpu.VMEM((TOK, HD), F32),
            pltpu.VMEM((1, HD), F32),
            pltpu.VMEM((1, D), F32),
            pltpu.VMEM((3, 704, 128), BF16),
            pltpu.VMEM((2 * D, 1408), BF16),
            pltpu.VMEM((32, 704, 128), BF16),
            pltpu.VMEM((8, 1024, 256), BF16),
            pltpu.VMEM((4, 128, D), BF16),
            pltpu.VMEM((8, ROWS, 128), BF16),
            pltpu.VMEM((2, ROWS, 128), BF16),
            pltpu.VMEM((8, ROWS, 256), BF16),
            pltpu.VMEM((8, ROWS, 256), BF16),
            pltpu.VMEM((11, ROWS, 256), F32),
            pltpu.VMEM((11, ROWS, 128), BF16),
            pltpu.VMEM((ROWS, 128), F32),
            pltpu.VMEM((2, ROWS, 256), F32),
            pltpu.VMEM((TOK, HD), F32),
            pltpu.VMEM((TOK, HD), F32),
            pltpu.VMEM((16, HD, HD), F32),
            pltpu.VMEM((16, HD, HD), BF16),
            pltpu.VMEM((4, 144, HD), BF16),
            pltpu.VMEM((4, 144, HD), BF16),
            pltpu.VMEM((TOK, HD), F32),
            pltpu.VMEM((TOK, HD), BF16),
            pltpu.VMEM((TOK, HD), F32),
            pltpu.VMEM((8, 2, 128, 128), BF16),
            pltpu.VMEM((8, 2, 128, 128), BF16),
            pltpu.VMEM((8, 128, 256), F32),
            pltpu.VMEM((2, 8, 128, 256), F32),
            pltpu.VMEM((8, 2, 128, 256), BF16),
            pltpu.VMEM((8, 2, 128, 256), BF16),
            dma((2, 10)),
            dma((4,)),
            dma((8,)),
            dma((2,)),
            dma((3,)),
            dma((1,)),
            dma((3,)),
            dma((3,)),
            dma((4,)),
            dma((1,)),
            dma((7,)),
            dma((1,)),
            dma((1,)),
            dma((8,)),
            dma((8,)),
            dma((1,)),
            dma((8,)),
            dma((1,)),
        ],
        compiler_params=pltpu.CompilerParams(
            collective_id=0, has_side_effects=True, vmem_limit_bytes=58000000
        ),
        name="layer",
    )(
        skip, q, r, v, e, slack.reshape(1, -1), surge, gain.reshape(1, -1), emission,
        norm_gain.reshape(1, -1), gate.T, up.T, down,
    )


def solution(mesh):
    split = Mesh(mesh.devices.reshape(4, 4, 4, 2), ("z", "y", "x", "c"))
    sp, tp = ("z", "y"), ("x", "c")
    return jax.shard_map(
        on_device,
        mesh=split,
        in_specs=(
            P(sp + tp, None),
            P(sp, tp),
            P(sp, tp),
            P(sp, tp),
            P(sp, tp),
            P(tp),
            P(sp, tp),
            P(tp),
            P(),
            P(),
            P(sp, tp),
            P(sp, tp),
            P(tp, sp),
        ),
        out_specs=P(sp + tp, None),
        check_vma=False,
    )
```

time: 98.6 us -> 80.9 us (0.82)
  Pallas kernels: 91.7 us -> 78.3 us
  local copies, waits for them, and re-layouts: 5.35 us -> 1.88 us
    pallas_call x1, Pallas kernels: 91.7 us -> 78.3 us  [on_device(): pl.pallas_call(kernel, out_shape=jax.ShapeDtypeStruct((128, D), BF16), in...]
    unnamed x3 -> x1, local copies, waits for them, and re-layouts: 5.35 us -> 1.88 us
where the time goes in v2:
time: 80.9 us; the launch traced here: 80.2 us
  Pallas kernels  78.3 us (97%)
  local copies, waits for them, and re-layouts  1.88 us (2%)
    pallas_call x1, Pallas kernels, on_device(): pl.pallas_call(kernel, out_shape=jax.ShapeDtypeStruct((128, D), BF16), in...  78.3 us
    unnamed x1, local copies, waits for them, and re-layouts  1.88 us

profile of v2, /device:TPU:0, one launch (start us, length us, event | category | flops | bytes accessed | tf_op | source)
XLA Modules:
  0.0 80.2 jit_solution(14106787553108695792)
XLA Ops:
  0.0 78.3 %layer.1 = bf16[128,2048]{1,0:T(8,128)(2,1)} custom-call(bf16[128,2048]{1,0:T(8,128)(2,1)} %skip_in.1, bf16[1024,128]{1,0:T(8,128)(2,1)} %q_in.1, bf16[1024,128]{1,0:T(8,128)(2,1)} %r_in.1, bf16[1024,128]{1,0:T(8,128)(2,1)} %v_in.1, bf16[1024,128]{1,0:T(8,128)(2,1)} %e_in.1, f32[1,128]{1,0:T(1,128)} %bitcast.8, f32[1024,128]{1,0:T(8,128)} %surge_in.1, ...), custom_call_target="tpu_custom_call" | custom-call | tf_op jit(solution)/shard_map/layer/pallas_call | solution.py:585
  78.3 1.9 %copy.15 = bf16[128,2048]{1,0:T(8,128)(2,1)} copy(bf16[128,2048]{1,0:T(8,128)(2,1)} %layer.1) | data formatting | bytes 1048576

commit v3 on v2

--- a/solution.py
+++ b/solution.py
@@ -81,9 +81,6 @@
     load(e_in, e_ref, 5)
     load(gain_in, gain_ref, 6)
     load(norm_gain_in, norm_gain_ref, 7)
-    for n in range(8):
-        source = emission_ref.at[:, pl.ds(n * 256, 256)]
-        pltpu.make_async_copy(source, EB.at[n], e_sem.at[0]).start()
 
     arrive(OWNED, in_sem.at[0])
     own_rows = pl.ds(pl.multiple_of(c * D + sp * 128, 128), 128)
@@ -92,15 +89,138 @@
         W[own_rows, j * 256 + 128 : (j + 1) * 256] = up_ref[j * 128 : (j + 1) * 128].T
     W[own_rows, 1280:1408] = jnp.concatenate([gate_ref[640:704], up_ref[640:704]], axis=0).T
     DN[c * 16 + sp] = down_ref[...]
-    arrive(RV, in_sem.at[1])
-    arrive(surge_ref, in_sem.at[2])
-    arrive(slack_ref, in_sem.at[3])
+
+    pl.semaphore_wait(barrier, 11)
+
+    AXES = {0: ("y", "z"), 1: ("z", "y")}
+    ORDER = (
+        (0, 0), (1, 0), (-1, 0), (0, 1), (0, -1), (2, 0), (0, 2), (1, 1),
+        (-1, -1), (1, -1), (-1, 1), (2, 1), (2, -1), (1, 2), (-1, 2), (2, 2),
+    )
+    here = {"z": z, "y": y}
+
+    def short(offset):
+        return (offset + 1) % 4 - 1
+
+    def unit(kind, color, rel):
+        origin = wrap(z + rel["z"]) * 4 + wrap(y + rel["y"])
+        if kind == GU:
+            start = pl.multiple_of(c * D + origin * 128 + color * 64, 64)
+            return W.at[pl.ds(start, 64), :]
+        return DN.at[c * 16 + origin, pl.ds(color * 352, 352), :]
+
+    def units(kind, count):
+        return W.at[pl.ds(0, 64 * count), :] if kind == GU else DN.at[pl.ds(0, count // 2)]
+
+    counts = {GU: 0, DOWN: 0}
+
+    def lot(kind, color, rel):
+        one, two = AXES[color]
+        first, second = short(rel[one]), short(rel[two])
+        if second == 0:
+            return {-PLUS[kind]: 0, PLUS[kind]: 1, 2: 3}[first]
+        if second == 2:
+            return {0: 6, -1: 8, 1: 8, 2: 9}[first]
+        return {0: 2, -1: 4, 1: 5, 2: 7}[first]
+
+    LOTS = (2, 2, 4, 2, 4, 4, 2, 4, 4, 2)
+
+    def arrived(kind, number):
+        arrive(units(kind, LOTS[number]), w_recv.at[kind, number])
+
+    def start_unit(kind, color, rel, recv_sem, device):
+        ref = unit(kind, color, rel)
+        pltpu.make_async_remote_copy(
+            src_ref=ref, dst_ref=ref, send_sem=w_send.at[kind], recv_sem=recv_sem,
+            device_id=device, device_id_type=MESH,
+        ).start()
+        counts[kind] += 1
+
+    def push(kind, color, rel, axis, step):
+        there = dict(rel)
+        there[axis] = rel[axis] - step
+        sem = w_recv.at[kind, lot(kind, color, there)]
+        start_unit(kind, color, rel, sem, {axis: wrap(here[axis] + step)})
+
+    def side(kind, color, rel):
+        place = (short(rel["y"]), short(rel["z"]))
+        sem = side_gu.at[place[1] % 4] if kind == GU else side_down.at[ORDER.index(place) // 2]
+        start_unit(kind, color, rel, sem, {"c": other})
+
+    def at(color, first, second):
+        one, two = AXES[color]
+        return {one: first, two: second}
+
+    def turn(kind, second_offset):
+        return PLUS[kind] * {0: 1, -1: -1, 1: 1, 2: -1}[second_offset]
+
+    def stage(kind, n):
+        if n in (0, 1):
+            for color in (0, 1):
+                for step in (1, -1):
+                    push(kind, color, at(color, 0, 0), AXES[color][n], step)
+                if n == 1:
+                    side(kind, color, at(color, 0, 0))
+        if n == 2:
+            f = -PLUS[kind]
+            arrived(kind, 0)
+            for color in (0, 1):
+                push(kind, color, at(color, f, 0), AXES[color][0], -f)
+        for number, f in {2: ((0, -PLUS[kind]), (1, PLUS[kind])), 4: ((3, 2),)}.get(n, ()):
+            if number > 0:
+                arrived(kind, number)
+            for color in (0, 1):
+                for step in (1, -1):
+                    push(kind, color, at(color, f, 0), AXES[color][1], step)
+                side(kind, color, at(color, f, 0))
+        for number, first in {3: ((2, 0),), 5: ((4, -1),), 8: ((5, 1),), 6: ((7, 2),)}.get(n, ()):
+            arrived(kind, number)
+            for s in (-1, 1):
+                for color in (0, 1):
+                    if turn(kind, first) == -s:
+                        push(kind, color, at(color, first, s), AXES[color][1], -s)
+            for s in (-1, 1):
+                for color in (0, 1):
+                    side(kind, color, at(color, first, s))
+        for number, firsts in {8: ((6, (0,)),), 6: ((8, (-1, 1)),), 7: ((9, (2,)),)}.get(n, ()):
+            arrived(kind, number)
+            for first in firsts:
+                for color in (0, 1):
+                    side(kind, color, at(color, first, 2))
+
+    stage(GU, 0)
+
+    def skip_copy(source, slot, rows, sem, step):
+        return pltpu.make_async_remote_copy(
+            src_ref=source, dst_ref=SK.at[slot, rows, :],
+            send_sem=skip_send.at[0], recv_sem=skip_sem.at[sem],
+            device_id={"x": wrap(x + step)}, device_id_type=MESH,
+        )
+
+    arrive(skip_ref, in_sem.at[4])
+    for i, step in enumerate((1, -1)):
+        skip_copy(skip_ref, x, pl.ds(0, 128), i, step).start()
+
+    def skip_arrived(slot, rows, sem):
+        arrive(SK.at[slot, rows, :], skip_sem.at[sem])
+
+    def skip_relay(part):
+        left, right = wrap(x - 1), wrap(x + 1)
+        first, second = pl.ds(part * 32, 32), pl.ds(64 + part * 32, 32)
+        if part == 0:
+            skip_arrived(left, pl.ds(0, 128), 0)
+            skip_arrived(right, pl.ds(0, 128), 1)
+        skip_copy(SK.at[left, first, :], left, first, 2 + part, 1).start()
+        skip_copy(SK.at[right, second, :], right, second, 2 + part, -1).start()
 
     i256 = lax.broadcasted_iota(jnp.int32, (256, 256), 0)
     j256 = lax.broadcasted_iota(jnp.int32, (256, 256), 1)
     causal = jnp.logical_and(i256 >= j256, i256 // BLOCK == j256 // BLOCK)
     triangle = jnp.where(causal, 1.0, 0.0).astype(BF16)
     upper_half = lax.broadcasted_iota(jnp.int32, (128, 128), 0) < BLOCK
+    arrive(RV, in_sem.at[1])
+    arrive(surge_ref, in_sem.at[2])
+    arrive(slack_ref, in_sem.at[3])
     closings = []
     for s in range(4):
         rows = slice(s * 256, (s + 1) * 256)
@@ -153,8 +273,6 @@
 
     STR[0, 128:144] = spread(passed)
 
-    pl.semaphore_wait(barrier, 11)
-
     for k in range(1, 4):
         pltpu.make_async_remote_copy(
             src_ref=STR.at[0], dst_ref=STR.at[k],
@@ -162,158 +280,9 @@
             device_id={"y": wrap(y + k)}, device_id_type=MESH,
         ).start()
 
-    AXES = {0: ("y", "z"), 1: ("z", "y")}
-    ORDER = (
-        (0, 0), (1, 0), (-1, 0), (0, 1), (0, -1), (2, 0), (0, 2), (1, 1),
-        (-1, -1), (1, -1), (-1, 1), (2, 1), (2, -1), (1, 2), (-1, 2), (2, 2),
-    )
-    here = {"z": z, "y": y}
-
-    def short(offset):
-        return (offset + 1) % 4 - 1
-
-    def unit(kind, color, rel):
-        origin = wrap(z + rel["z"]) * 4 + wrap(y + rel["y"])
-        if kind == GU:
-            start = pl.multiple_of(c * D + origin * 128 + color * 64, 64)
-            return W.at[pl.ds(start, 64), :]
-        return DN.at[c * 16 + origin, pl.ds(color * 352, 352), :]
-
-    def units(kind, count):
-        return W.at[pl.ds(0, 64 * count), :] if kind == GU else DN.at[pl.ds(0, count // 2)]
-
-    counts = {GU: 0, DOWN: 0}
-
-    def lot(kind, color, rel):
-        one, two = AXES[color]
-        first, second = short(rel[one]), short(rel[two])
-        if second == 0:
-            return {-PLUS[kind]: 0, PLUS[kind]: 1, 2: 3}[first]
-        if second == 2:
-            return {0: 6, -1: 8, 1: 8, 2: 9}[first]
-        return {0: 2, -1: 4, 1: 5, 2: 7}[first]
-
-    LOTS = (2, 2, 4, 2, 4, 4, 2, 4, 4, 2)
-
-    def arrived(kind, number):
-        arrive(units(kind, LOTS[number]), w_recv.at[kind, number])
-
-    def start_unit(kind, color, rel, recv_sem, device):
-        ref = unit(kind, color, rel)
-        pltpu.make_async_remote_copy(
-            src_ref=ref, dst_ref=ref, send_sem=w_send.at[kind], recv_sem=recv_sem,
-            device_id=device, device_id_type=MESH,
-        ).start()
-        counts[kind] += 1
-
-    def push(kind, color, rel, axis, step):
-        there = dict(rel)
-        there[axis] = rel[axis] - step
-        sem = w_recv.at[kind, lot(kind, color, there)]
-        start_unit(kind, color, rel, sem, {axis: wrap(here[axis] + step)})
-
-    def side(kind, color, rel):
-        place = (short(rel["y"]), short(rel["z"]))
-        sem = side_gu.at[place[1] % 4] if kind == GU else side_down.at[ORDER.index(place) // 2]
-        start_unit(kind, color, rel, sem, {"c": other})
-
-    def at(color, first, second):
-        one, two = AXES[color]
-        return {one: first, two: second}
-
-    def turn(kind, second_offset):
-        return PLUS[kind] * {0: 1, -1: -1, 1: 1, 2: -1}[second_offset]
-
-    def stage(kind, n):
-        if n in (0, 1):
-            for color in (0, 1):
-                for step in (1, -1):
-                    push(kind, color, at(color, 0, 0), AXES[color][n], step)
-                if n == 1:
-                    side(kind, color, at(color, 0, 0))
-        if n == 2:
-            f = -PLUS[kind]
-            arrived(kind, 0)
-            for color in (0, 1):
-                push(kind, color, at(color, f, 0), AXES[color][0], -f)
-        for number, f in {2: ((0, -PLUS[kind]), (1, PLUS[kind])), 4: ((3, 2),)}.get(n, ()):
-            if number > 0:
-                arrived(kind, number)
-            for color in (0, 1):
-                for step in (1, -1):
-                    push(kind, color, at(color, f, 0), AXES[color][1], step)
-                side(kind, color, at(color, f, 0))
-        for number, first in {3: ((2, 0),), 5: ((4, -1), (5, 1)), 6: ((7, 2),)}.get(n, ()):
-            arrived(kind, number)
-            for s in (-1, 1):
-                for color in (0, 1):
-                    if turn(kind, first) == -s:
-                        push(kind, color, at(color, first, s), AXES[color][1], -s)
-            for s in (-1, 1):
-                for color in (0, 1):
-                    side(kind, color, at(color, first, s))
-        for number, firsts in {5: ((6, (0,)),), 6: ((8, (-1, 1)),), 7: ((9, (2,)),)}.get(n, ()):
-            arrived(kind, number)
-            for first in firsts:
-                for color in (0, 1):
-                    side(kind, color, at(color, first, 2))
-
-    stage(GU, 0)
-
-    def skip_copy(source, slot, rows, sem, step):
-        return pltpu.make_async_remote_copy(
-            src_ref=source, dst_ref=SK.at[slot, rows, :],
-            send_sem=skip_send.at[0], recv_sem=skip_sem.at[sem],
-            device_id={"x": wrap(x + step)}, device_id_type=MESH,
-        )
-
-    arrive(skip_ref, in_sem.at[4])
-    for i, step in enumerate((1, -1)):
-        skip_copy(skip_ref, x, pl.ds(0, 128), i, step).start()
-
-    def skip_arrived(slot, rows, sem):
-        arrive(SK.at[slot, rows, :], skip_sem.at[sem])
-
-    def skip_relay():
-        left, right = wrap(x - 1), wrap(x + 1)
-        first, second = pl.ds(0, 64), pl.ds(64, 64)
-        skip_arrived(left, pl.ds(0, 128), 0)
-        skip_copy(SK.at[left, first, :], left, first, 2, 1).start()
-        skip_arrived(right, pl.ds(0, 128), 1)
-        skip_copy(SK.at[right, second, :], right, second, 3, -1).start()
-
-    for k in range(1, 4):
-        arrive(STR.at[k], state_recv.at[k - 1])
-    plane = jnp.zeros((HD, HD), F32)
-    plane_log = jnp.zeros((1, HD), F32)
-    before, before_log = plane, plane_log
-    for yy in range(4):
-        slot = wrap(y - yy)
-        before = jnp.where(y == yy, plane, before)
-        before_log = jnp.where(y == yy, plane_log, before_log)
-        log = joined(STR[slot, 128:144])
-        plane = plane * jnp.exp(log) + STR[slot, 0:128].astype(F32)
-        plane_log = plane_log + log
-    TOT[0, 0:128] = plane.astype(BF16)
-    TOT[0, 128:144] = spread(plane_log)
-
-    def total_copy(k):
-        return pltpu.make_async_remote_copy(
-            src_ref=TOT.at[0], dst_ref=TOT.at[k],
-            send_sem=total_send.at[k - 1], recv_sem=total_recv.at[k - 1],
-            device_id={"z": wrap(z + k)}, device_id_type=MESH,
-        )
-
-    for k in range(1, 4):
-
-        @pl.when(z + k < 4)
-        def _():
-            total_copy(k).start()
-
-        @pl.when(z < k)
-        def _():
-            TOT[k] = jnp.zeros((144, HD), BF16)
-
+    for n in range(8):
+        source = emission_ref.at[:, pl.ds(n * 256, 256)]
+        pltpu.make_async_copy(source, EB.at[n], e_sem.at[0]).start()
     stage(GU, 1)
     SK[x] = skip_ref[...]
     arrive(QE, in_sem.at[5])
@@ -349,6 +318,39 @@
         GT[rows] = gain_ref[...] * emission * jax.nn.sigmoid(emission)
 
     for k in range(1, 4):
+        arrive(STR.at[k], state_recv.at[k - 1])
+    plane = jnp.zeros((HD, HD), F32)
+    plane_log = jnp.zeros((1, HD), F32)
+    before, before_log = plane, plane_log
+    for yy in range(4):
+        slot = wrap(y - yy)
+        before = jnp.where(y == yy, plane, before)
+        before_log = jnp.where(y == yy, plane_log, before_log)
+        log = joined(STR[slot, 128:144])
+        plane = plane * jnp.exp(log) + STR[slot, 0:128].astype(F32)
+        plane_log = plane_log + log
+    TOT[0, 0:128] = plane.astype(BF16)
+    TOT[0, 128:144] = spread(plane_log)
+
+    def total_copy(k):
+        return pltpu.make_async_remote_copy(
+            src_ref=TOT.at[0], dst_ref=TOT.at[k],
+            send_sem=total_send.at[k - 1], recv_sem=total_recv.at[k - 1],
+            device_id={"z": wrap(z + k)}, device_id_type=MESH,
+        )
+
+    for k in range(1, 4):
+
+        @pl.when(z + k < 4)
+        def _():
+            total_copy(k).start()
+
+        @pl.when(z < k)
+        def _():
+            TOT[k] = jnp.zeros((144, HD), BF16)
+
+    stage(GU, 2)
+    for k in range(1, 4):
 
         @pl.when(z >= k)
         def _():
@@ -385,39 +387,47 @@
     def mix_arrived(slab, sem):
         arrive(MX.at[slab], mix_recv.at[sem])
 
-    stage(GU, 2)
     stage(GU, 3)
-    skip_relay()
+    skip_relay(0)
     stage(GU, 4)
     left, right = wrap(x - 1), wrap(x + 1)
     mix_arrived(left * 2, 0)
     mix_copy(MX.at[left * 2], left * 2, 5, {"x": right})
     mix_arrived(right * 2 + 1, 3)
     mix_copy(MX.at[right * 2 + 1], right * 2 + 1, 6, {"x": left})
+    skip_relay(1)
     stage(GU, 5)
     arrive(EB, e_sem.at[0])
     opposite = wrap(x + 2)
-    skip_arrived(opposite, pl.ds(0, 64), 2)
-    skip_arrived(opposite, pl.ds(64, 64), 3)
     mix_arrived(left * 2 + 1, 1)
     mix_arrived(right * 2, 2)
     mix_arrived(x * 2 + other, 4)
     mix_arrived(opposite * 2, 5)
     mix_arrived(opposite * 2 + 1, 6)
 
-    SSQ[...] = jnp.zeros((ROWS, 128), F32)
-
     def project(n, carry):
         mixed = jnp.concatenate([MX[h] for h in range(8)], axis=1)
+        ACC[n] = mm(mixed, EB[n])
+        return carry
+
+    lax.fori_loop(0, 4, project, 0, unroll=True)
+    stage(GU, 8)
+    lax.fori_loop(4, 8, project, 0, unroll=True)
+    stage(DOWN, 0)
+    skip_arrived(opposite, pl.ds(0, 64), 2)
+    skip_arrived(opposite, pl.ds(64, 64), 3)
+    SSQ[...] = jnp.zeros((ROWS, 128), F32)
+
+    def add(n, carry):
         skipped = SK[:, :, pl.ds(pl.multiple_of(n * 256, 256), 256)].reshape(ROWS, 256)
-        stream = (skipped.astype(F32) + mm(mixed, EB[n])).astype(BF16)
+        stream = (skipped.astype(F32) + ACC[n]).astype(BF16)
         STREAM[n] = stream
         wide = stream.astype(F32)
         wide = wide * wide
         SSQ[...] += wide[:, :128] + wide[:, 128:]
         return carry
 
-    lax.fori_loop(0, 8, project, 0)
+    lax.fori_loop(0, 8, add, 0)
     scale = lax.rsqrt(jnp.sum(SSQ[...], axis=1, keepdims=True) * (1.0 / D) + EPSILON)
 
     for n in range(8):
@@ -432,7 +442,7 @@
     def silu(a):
         return a * jax.nn.sigmoid(a)
 
-    def gate_up(planes, first, last):
+    def gate_up(planes, first, last, begin=0, end=6):
         places = [wrap(z + dz) for dz in planes]
         rows = [
             [pl.ds(pl.multiple_of(h * D + p * 512, 512), 512) for p in places] for h in (0, 1)
@@ -455,7 +465,9 @@
                     HID[t] = (silu(part[:, :128]) * part[:, 128:]).astype(BF16)
             return carry
 
-        lax.fori_loop(0, 5, tile, 0)
+        lax.fori_loop(begin, min(end, 5), tile, 0, unroll=True)
+        if end < 6:
+            return
         part = partial(
             [
                 jnp.concatenate([W[one, 1280:1408], W[two, 1280:1408]], axis=1)
@@ -527,43 +539,48 @@
             columns = pl.ds(pl.multiple_of(column * 128, 128), 128)
             out_ref[:, columns] = (stream + summed[:, half * 128 : (half + 1) * 128]).astype(BF16)
 
-    stage(DOWN, 0)
+    stage(DOWN, 1)
     await_sides(0)
     gate_up((0,), True, False)
     stage(GU, 6)
-    stage(DOWN, 1)
     await_sides(-1)
     await_sides(1)
-    gate_up((-1, 1), False, False)
     stage(DOWN, 2)
+    gate_up((-1, 1), False, False, 0, 3)
+    stage(DOWN, 3)
+    gate_up((-1, 1), False, False, 3, 6)
     stage(GU, 7)
-    stage(DOWN, 3)
     await_sides(2)
+    stage(DOWN, 4)
     gate_up((2,), False, True)
     down(0)
-    stage(DOWN, 4)
+    stage(DOWN, 5)
     down(1)
-    stage(DOWN, 5)
+    stage(DOWN, 8)
     down(2)
     hand_on(0)
+    stage(DOWN, 6)
     down(3)
     hand_on(1)
     down(4)
-    stage(DOWN, 6)
     hand_on(2)
+    stage(DOWN, 7)
     down(5)
     hand_on(3)
     down(6)
-    stage(DOWN, 7)
     hand_on(4)
     down(7)
     hand_on(5)
     finish(0)
+    hand_on(6)
     finish(1)
-    hand_on(6)
+    finish(2)
     hand_on(7)
-    for i in range(2, 8):
-        finish(i)
+    finish(3)
+    finish(4)
+    finish(5)
+    finish(6)
+    finish(7)
 
     for kind in (GU, DOWN):
         arrive(units(kind, counts[kind]), w_send.at[kind])
@@ -643,12 +660,15 @@
             dma((1,)),
         ],
         compiler_params=pltpu.CompilerParams(
-            collective_id=0, has_side_effects=True, vmem_limit_bytes=58000000
+            collective_id=0, has_side_effects=True, vmem_limit_bytes=54000000
         ),
         name="layer",
     )(
-        skip, q, r, v, e, slack.reshape(1, -1), surge, gain.reshape(1, -1), emission,
-        norm_gain.reshape(1, -1), gate.T, up.T, down,
+        *(
+            pltpu.with_memory_space_constraint(a, pltpu.HBM)
+            for a in (skip, q, r, v, e, slack.reshape(1, -1), surge, gain.reshape(1, -1), emission,
+                      norm_gain.reshape(1, -1), gate.T, up.T, down)
+        )
     )
 
 

time: 80.9 us -> 76.8 us (0.949)
  Pallas kernels: 78.3 us -> 75.2 us
  local copies, waits for them, and re-layouts: 1.88 us -> 0.8 us
    pallas_call x1, Pallas kernels: 78.3 us -> 75.2 us  [on_device(): pl.pallas_call(kernel, out_shape=jax.ShapeDtypeStruct((128, D), BF16), in...]
    unnamed x1, local copies, waits for them, and re-layouts: 1.88 us -> 0.8 us
where the time goes in v3:
time: 76.8 us; the launch traced here: 76 us
  Pallas kernels  75.2 us (98%)
  local copies, waits for them, and re-layouts  0.8 us (1%)
    pallas_call x1, Pallas kernels, on_device(): pl.pallas_call(kernel, out_shape=jax.ShapeDtypeStruct((128, D), BF16), in...  75.2 us

profile of v3, /device:TPU:0, one launch (start us, length us, event | category | flops | bytes accessed | tf_op | source)
XLA Modules:
  0.0 76.0 jit_solution(4658379622450244347)
XLA Ops:
  0.0 75.2 %layer.1 = bf16[128,2048]{1,0:T(8,128)(2,1)S(1)} custom-call(bf16[128,2048]{1,0:T(8,128)(2,1)} %skip_in.1, bf16[1024,128]{1,0:T(8,128)(2,1)} %q_in.1, bf16[1024,128]{1,0:T(8,128)(2,1)} %r_in.1, bf16[1024,128]{1,0:T(8,128)(2,1)} %v_in.1, bf16[1024,128]{1,0:T(8,128)(2,1)} %e_in.1, f32[1,128]{1,0:T(1,128)} %bitcast.8, f32[1024,128]{1,0:T(8,128)} %surge_in.1, ...), custom_call_target="tpu_custom_call" | custom-call | tf_op jit(solution)/shard_map/layer/pallas_call | solution.py:602
  75.2 0.8 %copy.15 = bf16[128,2048]{1,0:T(8,128)(2,1)} copy(bf16[128,2048]{1,0:T(8,128)(2,1)S(1)} %layer.1) | data formatting | bytes 1048576

commit v4 on v3

--- a/solution.py
+++ b/solution.py
@@ -18,7 +18,6 @@
 ROWS = 512
 D = 2048
 GU, DOWN = 0, 1
-PLUS = {GU: +1, DOWN: -1}
 
 
 def wrap(value, n=4):
@@ -102,23 +101,24 @@
     def short(offset):
         return (offset + 1) % 4 - 1
 
-    def unit(kind, color, rel):
+    def unit(kind, color, rel, half):
         origin = wrap(z + rel["z"]) * 4 + wrap(y + rel["y"])
+        size, skipped = (1, 0) if half is None else (2, half)
         if kind == GU:
-            start = pl.multiple_of(c * D + origin * 128 + color * 64, 64)
-            return W.at[pl.ds(start, 64), :]
-        return DN.at[c * 16 + origin, pl.ds(color * 352, 352), :]
+            start = pl.multiple_of(c * D + origin * 128 + color * 64 + skipped * 32, 32)
+            return W.at[pl.ds(start, 64 // size), :]
+        return DN.at[c * 16 + origin, pl.ds(color * 352 + skipped * 176, 352 // size), :]
 
     def units(kind, count):
         return W.at[pl.ds(0, 64 * count), :] if kind == GU else DN.at[pl.ds(0, count // 2)]
 
     counts = {GU: 0, DOWN: 0}
 
-    def lot(kind, color, rel):
+    def lot(color, rel):
         one, two = AXES[color]
         first, second = short(rel[one]), short(rel[two])
         if second == 0:
-            return {-PLUS[kind]: 0, PLUS[kind]: 1, 2: 3}[first]
+            return {-1: 0, 1: 1, 2: 3}[first]
         if second == 2:
             return {0: 6, -1: 8, 1: 8, 2: 9}[first]
         return {0: 2, -1: 4, 1: 5, 2: 7}[first]
@@ -128,19 +128,19 @@
     def arrived(kind, number):
         arrive(units(kind, LOTS[number]), w_recv.at[kind, number])
 
-    def start_unit(kind, color, rel, recv_sem, device):
-        ref = unit(kind, color, rel)
+    def start_unit(kind, color, rel, recv_sem, device, half=None):
+        ref = unit(kind, color, rel, half)
         pltpu.make_async_remote_copy(
             src_ref=ref, dst_ref=ref, send_sem=w_send.at[kind], recv_sem=recv_sem,
             device_id=device, device_id_type=MESH,
         ).start()
-        counts[kind] += 1
-
-    def push(kind, color, rel, axis, step):
+        counts[kind] += 2 if half is None else 1
+
+    def push(kind, color, rel, axis, step, half=None):
         there = dict(rel)
         there[axis] = rel[axis] - step
-        sem = w_recv.at[kind, lot(kind, color, there)]
-        start_unit(kind, color, rel, sem, {axis: wrap(here[axis] + step)})
+        sem = w_recv.at[kind, lot(color, there)]
+        start_unit(kind, color, rel, sem, {axis: wrap(here[axis] + step)}, half)
 
     def side(kind, color, rel):
         place = (short(rel["y"]), short(rel["z"]))
@@ -150,9 +150,6 @@
     def at(color, first, second):
         one, two = AXES[color]
         return {one: first, two: second}
-
-    def turn(kind, second_offset):
-        return PLUS[kind] * {0: 1, -1: -1, 1: 1, 2: -1}[second_offset]
 
     def stage(kind, n):
         if n in (0, 1):
@@ -162,13 +159,14 @@
                 if n == 1:
                     side(kind, color, at(color, 0, 0))
         if n == 2:
-            f = -PLUS[kind]
             arrived(kind, 0)
-            for color in (0, 1):
-                push(kind, color, at(color, f, 0), AXES[color][0], -f)
-        for number, f in {2: ((0, -PLUS[kind]), (1, PLUS[kind])), 4: ((3, 2),)}.get(n, ()):
-            if number > 0:
-                arrived(kind, number)
+            arrived(kind, 1)
+            for f in (-1, 1):
+                for color in (0, 1):
+                    push(kind, color, at(color, f, 0), AXES[color][0], -f, (f + 1) // 2)
+        if n == 4:
+            arrived(kind, 3)
+        for f in {2: (-1, 1), 4: (2,)}.get(n, ()):
             for color in (0, 1):
                 for step in (1, -1):
                     push(kind, color, at(color, f, 0), AXES[color][1], step)
@@ -177,8 +175,7 @@
             arrived(kind, number)
             for s in (-1, 1):
                 for color in (0, 1):
-                    if turn(kind, first) == -s:
-                        push(kind, color, at(color, first, s), AXES[color][1], -s)
+                    push(kind, color, at(color, first, s), AXES[color][1], -s, (s + 1) // 2)
             for s in (-1, 1):
                 for color in (0, 1):
                     side(kind, color, at(color, first, s))
@@ -397,6 +394,7 @@
     mix_copy(MX.at[right * 2 + 1], right * 2 + 1, 6, {"x": left})
     skip_relay(1)
     stage(GU, 5)
+    stage(GU, 8)
     arrive(EB, e_sem.at[0])
     opposite = wrap(x + 2)
     mix_arrived(left * 2 + 1, 1)
@@ -411,7 +409,6 @@
         return carry
 
     lax.fori_loop(0, 4, project, 0, unroll=True)
-    stage(GU, 8)
     lax.fori_loop(4, 8, project, 0, unroll=True)
     stage(DOWN, 0)
     skip_arrived(opposite, pl.ds(0, 64), 2)
@@ -583,7 +580,7 @@
     finish(7)
 
     for kind in (GU, DOWN):
-        arrive(units(kind, counts[kind]), w_send.at[kind])
+        arrive(units(kind, counts[kind] // 2), w_send.at[kind])
     arrive(STR.at[pl.ds(0, 3)], state_send.at[0])
     arrive(SK.at[pl.ds(0, 3)], skip_send.at[0])
     arrive(MX.at[pl.ds(0, 7)], mix_send.at[0])

time: 76.8 us -> 72.5 us (0.944)
  Pallas kernels: 75.2 us -> 71.5 us
    pallas_call x1, Pallas kernels: 75.2 us -> 71.5 us  [on_device(): pl.pallas_call(kernel, out_shape=jax.ShapeDtypeStruct((128, D), BF16), in...]
where the time goes in v4:
time: 72.5 us; the launch traced here: 72.4 us
  Pallas kernels  71.5 us (99%)
  local copies, waits for them, and re-layouts  0.8 us (1%)
    pallas_call x1, Pallas kernels, on_device(): pl.pallas_call(kernel, out_shape=jax.ShapeDtypeStruct((128, D), BF16), in...  71.5 us

profile of v4, /device:TPU:0, one launch (start us, length us, event | category | flops | bytes accessed | tf_op | source)
XLA Modules:
  0.0 72.4 jit_solution(5622847554320898261)
XLA Ops:
  0.0 71.5 %layer.1 = bf16[128,2048]{1,0:T(8,128)(2,1)S(1)} custom-call(bf16[128,2048]{1,0:T(8,128)(2,1)} %skip_in.1, bf16[1024,128]{1,0:T(8,128)(2,1)} %q_in.1, bf16[1024,128]{1,0:T(8,128)(2,1)} %r_in.1, bf16[1024,128]{1,0:T(8,128)(2,1)} %v_in.1, bf16[1024,128]{1,0:T(8,128)(2,1)} %e_in.1, f32[1,128]{1,0:T(1,128)} %bitcast.8, f32[1024,128]{1,0:T(8,128)} %surge_in.1, ...), custom_call_target="tpu_custom_call" | custom-call | tf_op jit(solution)/shard_map/layer/pallas_call | solution.py:599
  71.6 0.8 %copy.15 = bf16[128,2048]{1,0:T(8,128)(2,1)} copy(bf16[128,2048]{1,0:T(8,128)(2,1)S(1)} %layer.1) | data formatting | bytes 1048576

commit v5 on v4

--- a/solution.py
+++ b/solution.py
@@ -434,19 +434,32 @@
     def await_sides(dz):
         arrive(units(GU, 8), side_gu.at[dz % 4])
 
-    lane = lax.broadcasted_iota(jnp.int32, (ROWS, 128), 1)
+    def chunk(xi):
+        return pl.ds(pl.multiple_of(xi * 128, 128), 128)
 
     def silu(a):
         return a * jax.nn.sigmoid(a)
 
-    def gate_up(planes, first, last, begin=0, end=6):
+    def gate_up(planes, first, last, begin=0, end=6, chunks=(0, 1, 2, 3)):
         places = [wrap(z + dz) for dz in planes]
         rows = [
             [pl.ds(pl.multiple_of(h * D + p * 512, 512), 512) for p in places] for h in (0, 1)
         ]
 
+        def some(ref, t):
+            if len(chunks) == 4:
+                return ref[t]
+            return jnp.concatenate([ref[t, chunk(wrap(x + k))] for k in chunks], axis=0)
+
+        def put(ref, t, value):
+            if len(chunks) == 4:
+                ref[t] = value
+                return
+            for n, k in enumerate(chunks):
+                ref[t, chunk(wrap(x + k))] = value[n * 128 : (n + 1) * 128]
+
         def partial(weights):
-            normed = [NORM[p * 2 + i] for p in places for i in (0, 1)]
+            normed = [some(NORM, p * 2 + i) for p in places for i in (0, 1)]
             return mm(jnp.concatenate(normed, axis=1), jnp.concatenate(weights, axis=0))
 
         def tile(j, carry):
@@ -455,11 +468,11 @@
                 t = h * 5 + j
                 part = partial([W[deep, columns] for deep in rows[h]])
                 if not first:
-                    part = part + ACC[t]
+                    part = part + some(ACC, t)
                 if not last:
-                    ACC[t] = part
+                    put(ACC, t, part)
                 else:
-                    HID[t] = (silu(part[:, :128]) * part[:, 128:]).astype(BF16)
+                    put(HID, t, (silu(part[:, :128]) * part[:, 128:]).astype(BF16))
             return carry
 
         lax.fori_loop(begin, min(end, 5), tile, 0, unroll=True)
@@ -472,46 +485,60 @@
             ]
         )
         if not first:
-            part = part + ACC[10]
+            part = part + some(ACC, 10)
         if not last:
-            ACC[10] = part
+            put(ACC, 10, part)
         else:
+            lane = lax.broadcasted_iota(jnp.int32, (128 * len(chunks), 128), 1)
             a, b = part[:, :128], part[:, 128:]
             gates = jnp.where(lane < 64, a, pltpu.roll(b, 64, 1))
             ups = jnp.where(lane < 64, pltpu.roll(a, 64, 1), b)
-            HID[10] = (silu(gates) * ups).astype(BF16)
-
-    def chunk(xi):
-        return pl.ds(pl.multiple_of(xi * 128, 128), 128)
+            put(HID, 10, (silu(gates) * ups).astype(BF16))
 
     def column_of(i):
         dy, dz = ORDER[i]
         return wrap(z + dz) * 4 + wrap(y + dy)
 
-    def down(i):
-        arrive(units(DOWN, 4), side_down.at[i])
-
+    def down_weights(i):
         def block(at_column):
             one, two = at_column, 16 + at_column
             return jnp.concatenate(
                 [DN[one, 0:640], DN[two, 0:640], DN[one, 640:704], DN[two, 640:704]], axis=0
             )
 
-        weights = jnp.concatenate([block(column_of(2 * i)), block(column_of(2 * i + 1))], axis=1)
-        hidden = jnp.concatenate([HID[t] for t in range(11)], axis=1)
-        res = RES.at[i % 2]
-        res[...] = mm(hidden, weights)
-        far = res[chunk(opposite)].astype(BF16)
+        return jnp.concatenate([block(column_of(2 * i)), block(column_of(2 * i + 1))], axis=1)
+
+    def send_far(i, far):
         for half, step in enumerate((1, -1)):
-            OPPS[i, half] = far[:, half * 128 : (half + 1) * 128]
+            OPPS[i, half] = far[:, half * 128 : (half + 1) * 128].astype(BF16)
             pltpu.make_async_remote_copy(
                 src_ref=OPPS.at[i, half], dst_ref=OPPR.at[i, half],
                 send_sem=opp_send.at[0], recv_sem=opp_recv.at[i],
                 device_id={"x": wrap(x + step)}, device_id_type=MESH,
             ).start()
+
+    def down(i):
+        arrive(units(DOWN, 4), side_down.at[i])
+        res = RES.at[i % 2]
+        res[...] = mm(jnp.concatenate([HID[t] for t in range(11)], axis=1), down_weights(i))
+        send_far(i, res[chunk(opposite)])
         OWN[i] = res[chunk(x)]
         PN[0, i] = res[chunk(right)]
         PN[1, i] = res[chunk(left)]
+
+    def down_far(i):
+        arrive(units(DOWN, 4), side_down.at[i])
+        hidden = jnp.concatenate([HID[t, chunk(opposite)] for t in range(11)], axis=1)
+        send_far(i, mm(hidden, down_weights(i)))
+
+    def down_near(i):
+        hidden = [
+            jnp.concatenate([HID[t, chunk(k)] for t in range(11)], axis=1) for k in (x, right, left)
+        ]
+        near = mm(jnp.concatenate(hidden, axis=0), down_weights(i))
+        OWN[i] = near[:128]
+        PN[0, i] = near[128:256]
+        PN[1, i] = near[256:]
 
     def hand_on(i):
         arrive(OPPR.at[i], opp_recv.at[i])
@@ -544,21 +571,24 @@
     await_sides(1)
     stage(DOWN, 2)
     gate_up((-1, 1), False, False, 0, 3)
+    stage(GU, 7)
     stage(DOWN, 3)
     gate_up((-1, 1), False, False, 3, 6)
-    stage(GU, 7)
     await_sides(2)
     stage(DOWN, 4)
-    gate_up((2,), False, True)
-    down(0)
+    gate_up((2,), False, True, chunks=(2,))
+    down_far(0)
+    down_far(1)
+    gate_up((2,), False, True, chunks=(0, 1, -1))
     stage(DOWN, 5)
-    down(1)
+    down_near(0)
     stage(DOWN, 8)
+    down_near(1)
+    hand_on(0)
     down(2)
-    hand_on(0)
     stage(DOWN, 6)
+    hand_on(1)
     down(3)
-    hand_on(1)
     down(4)
     hand_on(2)
     stage(DOWN, 7)

time: 72.5 us -> 71.2 us (0.982)
  Pallas kernels: 71.5 us -> 70.3 us
    pallas_call x1, Pallas kernels: 71.5 us -> 70.3 us  [on_device(): pl.pallas_call(kernel, out_shape=jax.ShapeDtypeStruct((128, D), BF16), in...]
where the time goes in v5:
time: 71.2 us; the launch traced here: 71.1 us
  Pallas kernels  70.3 us (99%)
  local copies, waits for them, and re-layouts  0.8 us (1%)
    pallas_call x1, Pallas kernels, on_device(): pl.pallas_call(kernel, out_shape=jax.ShapeDtypeStruct((128, D), BF16), in...  70.3 us

profile of v5, /device:TPU:0, one launch (start us, length us, event | category | flops | bytes accessed | tf_op | source)
XLA Modules:
  0.0 71.1 jit_solution(13700730378200156140)
XLA Ops:
  0.0 70.3 %layer.1 = bf16[128,2048]{1,0:T(8,128)(2,1)S(1)} custom-call(bf16[128,2048]{1,0:T(8,128)(2,1)} %skip_in.1, bf16[1024,128]{1,0:T(8,128)(2,1)} %q_in.1, bf16[1024,128]{1,0:T(8,128)(2,1)} %r_in.1, bf16[1024,128]{1,0:T(8,128)(2,1)} %v_in.1, bf16[1024,128]{1,0:T(8,128)(2,1)} %e_in.1, f32[1,128]{1,0:T(1,128)} %bitcast.8, f32[1024,128]{1,0:T(8,128)} %surge_in.1, ...), custom_call_target="tpu_custom_call" | custom-call | tf_op jit(solution)/shard_map/layer/pallas_call | solution.py:629
  70.3 0.8 %copy.15 = bf16[128,2048]{1,0:T(8,128)(2,1)} copy(bf16[128,2048]{1,0:T(8,128)(2,1)S(1)} %layer.1) | data formatting | bytes 1048576

commit v6 on v5

--- a/solution.py
+++ b/solution.py
@@ -93,8 +93,8 @@
 
     AXES = {0: ("y", "z"), 1: ("z", "y")}
     ORDER = (
-        (0, 0), (1, 0), (-1, 0), (0, 1), (0, -1), (2, 0), (0, 2), (1, 1),
-        (-1, -1), (1, -1), (-1, 1), (2, 1), (2, -1), (1, 2), (-1, 2), (2, 2),
+        (0, 0), (1, 0), (-1, 0), (0, 1), (0, -1), (-1, -1), (1, 1), (1, -1),
+        (-1, 1), (2, 0), (0, 2), (2, 1), (2, -1), (1, 2), (-1, 2), (2, 2),
     )
     here = {"z": z, "y": y}
 
@@ -185,7 +185,10 @@
                 for color in (0, 1):
                     side(kind, color, at(color, first, 2))
 
-    stage(GU, 0)
+    own = at(0, 0, 0)
+    for step in (1, -1):
+        push(GU, 0, own, "y", step, 0)
+        push(GU, 1, own, "z", step)
 
     def skip_copy(source, slot, rows, sem, step):
         return pltpu.make_async_remote_copy(
@@ -280,7 +283,10 @@
     for n in range(8):
         source = emission_ref.at[:, pl.ds(n * 256, 256)]
         pltpu.make_async_copy(source, EB.at[n], e_sem.at[0]).start()
-    stage(GU, 1)
+    for step in (1, -1):
+        push(GU, 0, own, "y", step, 1)
+        push(GU, 1, own, "y", step)
+        push(GU, 0, own, "z", step, 0)
     SK[x] = skip_ref[...]
     arrive(QE, in_sem.at[5])
     arrive(gain_ref, in_sem.at[6])
@@ -346,6 +352,10 @@
         def _():
             TOT[k] = jnp.zeros((144, HD), BF16)
 
+    for step in (1, -1):
+        push(GU, 0, own, "z", step, 1)
+    for color in (0, 1):
+        side(GU, color, own)
     stage(GU, 2)
     for k in range(1, 4):
 
@@ -395,6 +405,7 @@
     skip_relay(1)
     stage(GU, 5)
     stage(GU, 8)
+    stage(DOWN, 0)
     arrive(EB, e_sem.at[0])
     opposite = wrap(x + 2)
     mix_arrived(left * 2 + 1, 1)
@@ -410,7 +421,6 @@
 
     lax.fori_loop(0, 4, project, 0, unroll=True)
     lax.fori_loop(4, 8, project, 0, unroll=True)
-    stage(DOWN, 0)
     skip_arrived(opposite, pl.ds(0, 64), 2)
     skip_arrived(opposite, pl.ds(64, 64), 3)
     SSQ[...] = jnp.zeros((ROWS, 128), F32)
@@ -517,14 +527,27 @@
                 device_id={"x": wrap(x + step)}, device_id_type=MESH,
             ).start()
 
+    def send_half(i, half, columns):
+        pltpu.make_async_remote_copy(
+            src_ref=NBS.at[i, half, columns], dst_ref=NBR.at[i, half, columns],
+            send_sem=nb_send.at[0], recv_sem=nb_recv.at[i],
+            device_id={"x": wrap(x + 1 - 2 * half)}, device_id_type=MESH,
+        ).start()
+
+    def send_near(i, near):
+        for half in (0, 1):
+            rest = 1 - half
+            NBS[i, half, rest] = near[half][:, rest * 128 : (rest + 1) * 128].astype(BF16)
+            send_half(i, half, rest)
+            PN[half, i] = near[half][:, half * 128 : (half + 1) * 128]
+
     def down(i):
         arrive(units(DOWN, 4), side_down.at[i])
         res = RES.at[i % 2]
         res[...] = mm(jnp.concatenate([HID[t] for t in range(11)], axis=1), down_weights(i))
         send_far(i, res[chunk(opposite)])
         OWN[i] = res[chunk(x)]
-        PN[0, i] = res[chunk(right)]
-        PN[1, i] = res[chunk(left)]
+        send_near(i, (res[chunk(right)], res[chunk(left)]))
 
     def down_far(i):
         arrive(units(DOWN, 4), side_down.at[i])
@@ -537,31 +560,24 @@
         ]
         near = mm(jnp.concatenate(hidden, axis=0), down_weights(i))
         OWN[i] = near[:128]
-        PN[0, i] = near[128:256]
-        PN[1, i] = near[256:]
+        send_near(i, (near[128:256], near[256:]))
 
     def hand_on(i):
         arrive(OPPR.at[i], opp_recv.at[i])
-        for half, step in enumerate((1, -1)):
-            mine = slice(half * 128, (half + 1) * 128)
-            rest = slice(128 - half * 128, 256 - half * 128)
-            NBS[i, half, :, mine] = (PN[half, i, :, mine] + OPPR[i, half].astype(F32)).astype(BF16)
-            NBS[i, half, :, rest] = PN[half, i, :, rest].astype(BF16)
-            pltpu.make_async_remote_copy(
-                src_ref=NBS.at[i, half], dst_ref=NBR.at[i, half],
-                send_sem=nb_send.at[0], recv_sem=nb_recv.at[i],
-                device_id={"x": wrap(x + step)}, device_id_type=MESH,
-            ).start()
+        for half in (0, 1):
+            NBS[i, half, half] = (PN[half, i] + OPPR[i, half].astype(F32)).astype(BF16)
+            send_half(i, half, half)
 
     def finish(i):
         arrive(NBR.at[i], nb_recv.at[i])
-        summed = OWN[i] + NBR[i, 0].astype(F32) + NBR[i, 1].astype(F32)
         for half in (0, 1):
             column = column_of(2 * i + half)
             lanes = pl.ds(pl.multiple_of(lax.rem(column, 2) * 128, 128), 128)
             stream = STREAM[column // 2, chunk(x), lanes].astype(F32)
+            summed = OWN[i, :, half * 128 : (half + 1) * 128]
+            summed = summed + NBR[i, 0, half].astype(F32) + NBR[i, 1, half].astype(F32)
             columns = pl.ds(pl.multiple_of(column * 128, 128), 128)
-            out_ref[:, columns] = (stream + summed[:, half * 128 : (half + 1) * 128]).astype(BF16)
+            out_ref[:, columns] = (stream + summed).astype(BF16)
 
     stage(DOWN, 1)
     await_sides(0)
@@ -575,25 +591,25 @@
     stage(DOWN, 3)
     gate_up((-1, 1), False, False, 3, 6)
     await_sides(2)
-    stage(DOWN, 4)
     gate_up((2,), False, True, chunks=(2,))
     down_far(0)
     down_far(1)
+    stage(DOWN, 4)
+    stage(DOWN, 5)
     gate_up((2,), False, True, chunks=(0, 1, -1))
-    stage(DOWN, 5)
     down_near(0)
     stage(DOWN, 8)
     down_near(1)
     hand_on(0)
     down(2)
+    down(3)
+    hand_on(1)
     stage(DOWN, 6)
-    hand_on(1)
-    down(3)
     down(4)
     hand_on(2)
-    stage(DOWN, 7)
     down(5)
     hand_on(3)
+    stage(DOWN, 7)
     down(6)
     hand_on(4)
     down(7)
@@ -664,9 +680,9 @@
             pltpu.VMEM((8, 2, 128, 128), BF16),
             pltpu.VMEM((8, 2, 128, 128), BF16),
             pltpu.VMEM((8, 128, 256), F32),
-            pltpu.VMEM((2, 8, 128, 256), F32),
-            pltpu.VMEM((8, 2, 128, 256), BF16),
-            pltpu.VMEM((8, 2, 128, 256), BF16),
+            pltpu.VMEM((2, 8, 128, 128), F32),
+            pltpu.VMEM((8, 2, 2, 128, 128), BF16),
+            pltpu.VMEM((8, 2, 2, 128, 128), BF16),
             dma((2, 10)),
             dma((4,)),
             dma((8,)),

time: 71.2 us -> 70.1 us (0.985)
  Pallas kernels: 70.3 us -> 69.2 us
    pallas_call x1, Pallas kernels: 70.3 us -> 69.2 us  [on_device(): pl.pallas_call(kernel, out_shape=jax.ShapeDtypeStruct((128, D), BF16), in...]
where the time goes in v6:
time: 70.1 us; the launch traced here: 70 us
  Pallas kernels  69.2 us (99%)
  local copies, waits for them, and re-layouts  0.8 us (1%)
    pallas_call x1, Pallas kernels, on_device(): pl.pallas_call(kernel, out_shape=jax.ShapeDtypeStruct((128, D), BF16), in...  69.2 us

profile of v6, /device:TPU:0, one launch (start us, length us, event | category | flops | bytes accessed | tf_op | source)
XLA Modules:
  0.0 70.0 jit_solution(4976054827593487835)
XLA Ops:
  0.0 69.2 %layer.1 = bf16[128,2048]{1,0:T(8,128)(2,1)S(1)} custom-call(bf16[128,2048]{1,0:T(8,128)(2,1)} %skip_in.1, bf16[1024,128]{1,0:T(8,128)(2,1)} %q_in.1, bf16[1024,128]{1,0:T(8,128)(2,1)} %r_in.1, bf16[1024,128]{1,0:T(8,128)(2,1)} %v_in.1, bf16[1024,128]{1,0:T(8,128)(2,1)} %e_in.1, f32[1,128]{1,0:T(1,128)} %bitcast.8, f32[1024,128]{1,0:T(8,128)} %surge_in.1, ...), custom_call_target="tpu_custom_call" | custom-call | tf_op jit(solution)/shard_map/layer/pallas_call | solution.py:645
  69.2 0.8 %copy.15 = bf16[128,2048]{1,0:T(8,128)(2,1)} copy(bf16[128,2048]{1,0:T(8,128)(2,1)S(1)} %layer.1) | data formatting | bytes 1048576

commit v7 on v6

--- a/solution.py
+++ b/solution.py
@@ -144,7 +144,11 @@
 
     def side(kind, color, rel):
         place = (short(rel["y"]), short(rel["z"]))
-        sem = side_gu.at[place[1] % 4] if kind == GU else side_down.at[ORDER.index(place) // 2]
+        if kind == GU:
+            late = (place[0] == 2) + (place[1] == 2)
+            sem = side_gu.at[1 if late == 1 and 0 not in place else late if 0 not in place else 0]
+        else:
+            sem = side_down.at[ORDER.index(place) // 2]
         start_unit(kind, color, rel, sem, {"c": other})
 
     def at(color, first, second):
@@ -406,6 +410,7 @@
     stage(GU, 5)
     stage(GU, 8)
     stage(DOWN, 0)
+    stage(DOWN, 1)
     arrive(EB, e_sem.at[0])
     opposite = wrap(x + 2)
     mix_arrived(left * 2 + 1, 1)
@@ -441,8 +446,8 @@
         gain = norm_gain_ref[:, n * 256 : (n + 1) * 256]
         NORM[n] = (STREAM[n].astype(F32) * scale * gain).astype(BF16)
 
-    def await_sides(dz):
-        arrive(units(GU, 8), side_gu.at[dz % 4])
+    def await_sides(group):
+        arrive(units(GU, (22, 8, 2)[group]), side_gu.at[group])
 
     def chunk(xi):
         return pl.ds(pl.multiple_of(xi * 128, 128), 128)
@@ -451,15 +456,24 @@
         return a * jax.nn.sigmoid(a)
 
     def gate_up(planes, first, last, begin=0, end=6, chunks=(0, 1, 2, 3)):
-        places = [wrap(z + dz) for dz in planes]
-        rows = [
-            [pl.ds(pl.multiple_of(h * D + p * 512, 512), 512) for p in places] for h in (0, 1)
-        ]
-
-        def some(ref, t):
+        tiles, rows = [], ([], [])
+        for part in planes:
+            if isinstance(part, int):
+                place = wrap(z + part)
+                tiles += [(place * 2, slice(None)), (place * 2 + 1, slice(None))]
+                start, size = place * 512, 512
+            else:
+                place = wrap(z + part[1]) * 4 + wrap(y + part[0])
+                lanes = pl.ds(pl.multiple_of(lax.rem(place, 2) * 128, 128), 128)
+                tiles.append((place // 2, lanes))
+                start, size = place * 128, 128
+            for h in (0, 1):
+                rows[h].append(pl.ds(pl.multiple_of(h * D + start, 128), size))
+
+        def some(ref, t, lanes=slice(None)):
             if len(chunks) == 4:
-                return ref[t]
-            return jnp.concatenate([ref[t, chunk(wrap(x + k))] for k in chunks], axis=0)
+                return ref[t, :, lanes]
+            return jnp.concatenate([ref[t, chunk(wrap(x + k)), lanes] for k in chunks], axis=0)
 
         def put(ref, t, value):
             if len(chunks) == 4:
@@ -469,7 +483,7 @@
                 ref[t, chunk(wrap(x + k))] = value[n * 128 : (n + 1) * 128]
 
         def partial(weights):
-            normed = [some(NORM, p * 2 + i) for p in places for i in (0, 1)]
+            normed = [some(NORM, t, lanes) for t, lanes in tiles]
             return mm(jnp.concatenate(normed, axis=1), jnp.concatenate(weights, axis=0))
 
         def tile(j, carry):
@@ -579,38 +593,37 @@
             columns = pl.ds(pl.multiple_of(column * 128, 128), 128)
             out_ref[:, columns] = (stream + summed).astype(BF16)
 
-    stage(DOWN, 1)
     await_sides(0)
-    gate_up((0,), True, False)
+    gate_up((0, (0, -1), (-1, -1), (1, -1), (0, 1), (-1, 1), (1, 1), (0, 2)), True, False, 0, 3)
     stage(GU, 6)
-    await_sides(-1)
+    gate_up((0, (0, -1), (-1, -1), (1, -1), (0, 1), (-1, 1), (1, 1), (0, 2)), True, False, 3, 6)
+    stage(DOWN, 2)
     await_sides(1)
-    stage(DOWN, 2)
-    gate_up((-1, 1), False, False, 0, 3)
+    gate_up(((2, -1), (2, 1), (-1, 2), (1, 2)), False, False, 0, 3)
     stage(GU, 7)
+    gate_up(((2, -1), (2, 1), (-1, 2), (1, 2)), False, False, 3, 6)
     stage(DOWN, 3)
-    gate_up((-1, 1), False, False, 3, 6)
     await_sides(2)
-    gate_up((2,), False, True, chunks=(2,))
+    gate_up(((2, 2),), False, True, chunks=(2,))
     down_far(0)
     down_far(1)
     stage(DOWN, 4)
+    gate_up(((2, 2),), False, True, chunks=(0, 1, -1))
+    down_near(0)
     stage(DOWN, 5)
-    gate_up((2,), False, True, chunks=(0, 1, -1))
-    down_near(0)
-    stage(DOWN, 8)
     down_near(1)
     hand_on(0)
+    stage(DOWN, 8)
     down(2)
     down(3)
     hand_on(1)
+    down(4)
     stage(DOWN, 6)
-    down(4)
     hand_on(2)
     down(5)
     hand_on(3)
+    down(6)
     stage(DOWN, 7)
-    down(6)
     hand_on(4)
     down(7)
     hand_on(5)
@@ -684,7 +697,7 @@
             pltpu.VMEM((8, 2, 2, 128, 128), BF16),
             pltpu.VMEM((8, 2, 2, 128, 128), BF16),
             dma((2, 10)),
-            dma((4,)),
+            dma((3,)),
             dma((8,)),
             dma((2,)),
             dma((3,)),

time: 70.1 us -> 69.4 us (0.990)
  Pallas kernels: 69.2 us -> 68.4 us
    pallas_call x1, Pallas kernels: 69.2 us -> 68.4 us  [on_device(): pl.pallas_call(kernel, out_shape=jax.ShapeDtypeStruct((128, D), BF16), in...]
where the time goes in v7:
time: 69.4 us; the launch traced here: 69.2 us
  Pallas kernels  68.4 us (99%)
  local copies, waits for them, and re-layouts  0.8 us (1%)
    pallas_call x1, Pallas kernels, on_device(): pl.pallas_call(kernel, out_shape=jax.ShapeDtypeStruct((128, D), BF16), in...  68.4 us

profile of v7, /device:TPU:0, one launch (start us, length us, event | category | flops | bytes accessed | tf_op | source)
XLA Modules:
  0.0 69.2 jit_solution(2732407573807952349)
XLA Ops:
  0.0 68.4 %layer.1 = bf16[128,2048]{1,0:T(8,128)(2,1)S(1)} custom-call(bf16[128,2048]{1,0:T(8,128)(2,1)} %skip_in.1, bf16[1024,128]{1,0:T(8,128)(2,1)} %q_in.1, bf16[1024,128]{1,0:T(8,128)(2,1)} %r_in.1, bf16[1024,128]{1,0:T(8,128)(2,1)} %v_in.1, bf16[1024,128]{1,0:T(8,128)(2,1)} %e_in.1, f32[1,128]{1,0:T(1,128)} %bitcast.8, f32[1024,128]{1,0:T(8,128)} %surge_in.1, ...), custom_call_target="tpu_custom_call" | custom-call | tf_op jit(solution)/shard_map/layer/pallas_call | solution.py:658
  68.5 0.8 %copy.15 = bf16[128,2048]{1,0:T(8,128)(2,1)} copy(bf16[128,2048]{1,0:T(8,128)(2,1)S(1)} %layer.1) | data formatting | bytes 1048576

commit v8 on v7

--- a/solution.py
+++ b/solution.py
@@ -601,8 +601,8 @@
     await_sides(1)
     gate_up(((2, -1), (2, 1), (-1, 2), (1, 2)), False, False, 0, 3)
     stage(GU, 7)
+    stage(DOWN, 3)
     gate_up(((2, -1), (2, 1), (-1, 2), (1, 2)), False, False, 3, 6)
-    stage(DOWN, 3)
     await_sides(2)
     gate_up(((2, 2),), False, True, chunks=(2,))
     down_far(0)

time: 69.4 us -> 69.1 us (level)
  no operation moved by 1% of the time
where the time goes in v8:
time: 69.1 us; the launch traced here: 68.7 us
  Pallas kernels  67.9 us (98%)
  local copies, waits for them, and re-layouts  0.8 us (1%)
    pallas_call x1, Pallas kernels, on_device(): pl.pallas_call(kernel, out_shape=jax.ShapeDtypeStruct((128, D), BF16), in...  67.9 us

profile of v8, /device:TPU:0, one launch (start us, length us, event | category | flops | bytes accessed | tf_op | source)
XLA Modules:
  0.0 68.7 jit_solution(8532721335560979396)
XLA Ops:
  0.0 67.9 %layer.1 = bf16[128,2048]{1,0:T(8,128)(2,1)S(1)} custom-call(bf16[128,2048]{1,0:T(8,128)(2,1)} %skip_in.1, bf16[1024,128]{1,0:T(8,128)(2,1)} %q_in.1, bf16[1024,128]{1,0:T(8,128)(2,1)} %r_in.1, bf16[1024,128]{1,0:T(8,128)(2,1)} %v_in.1, bf16[1024,128]{1,0:T(8,128)(2,1)} %e_in.1, f32[1,128]{1,0:T(1,128)} %bitcast.8, f32[1024,128]{1,0:T(8,128)} %surge_in.1, ...), custom_call_target="tpu_custom_call" | custom-call | tf_op jit(solution)/shard_map/layer/pallas_call | solution.py:658
  67.9 0.8 %copy.15 = bf16[128,2048]{1,0:T(8,128)(2,1)} copy(bf16[128,2048]{1,0:T(8,128)(2,1)S(1)} %layer.1) | data formatting | bytes 1048576

commit v9 on v8

--- a/solution.py
+++ b/solution.py
@@ -616,16 +616,16 @@
     stage(DOWN, 8)
     down(2)
     down(3)
+    down(4)
     hand_on(1)
-    down(4)
     stage(DOWN, 6)
     hand_on(2)
     down(5)
     hand_on(3)
     down(6)
     stage(DOWN, 7)
+    down(7)
     hand_on(4)
-    down(7)
     hand_on(5)
     finish(0)
     hand_on(6)

time: 69.1 us -> 68.5 us (level)
  no operation moved by 1% of the time
where the time goes in v9:
time: 68.5 us; the launch traced here: 68.2 us
  Pallas kernels  67.4 us (98%)
  local copies, waits for them, and re-layouts  0.8 us (1%)
    pallas_call x1, Pallas kernels, on_device(): pl.pallas_call(kernel, out_shape=jax.ShapeDtypeStruct((128, D), BF16), in...  67.4 us

profile of v9, /device:TPU:0, one launch (start us, length us, event | category | flops | bytes accessed | tf_op | source)
XLA Modules:
  0.0 68.2 jit_solution(15690659800989129197)
XLA Ops:
  0.0 67.4 %layer.1 = bf16[128,2048]{1,0:T(8,128)(2,1)S(1)} custom-call(bf16[128,2048]{1,0:T(8,128)(2,1)} %skip_in.1, bf16[1024,128]{1,0:T(8,128)(2,1)} %q_in.1, bf16[1024,128]{1,0:T(8,128)(2,1)} %r_in.1, bf16[1024,128]{1,0:T(8,128)(2,1)} %v_in.1, bf16[1024,128]{1,0:T(8,128)(2,1)} %e_in.1, f32[1,128]{1,0:T(1,128)} %bitcast.8, f32[1024,128]{1,0:T(8,128)} %surge_in.1, ...), custom_call_target="tpu_custom_call" | custom-call | tf_op jit(solution)/shard_map/layer/pallas_call | solution.py:658
  67.4 0.8 %copy.15 = bf16[128,2048]{1,0:T(8,128)(2,1)} copy(bf16[128,2048]{1,0:T(8,128)(2,1)S(1)} %layer.1) | data formatting | bytes 1048576
